TPU v7x, 128 devices: a whole 4x4x4 slice. The times are simulated.
128 devices in a mesh: sp: 16 (over z, x), tp: 8 (over y, core).
Axes of the slice: x: 4, y: 4, z: 4, core: 2. Of those that a mesh axis runs over, the one named last changes fastest.
Arguments:
- tokens: bfloat16 [6144, 2048], P('sp', 'tp'), may hold values from -6 to 6
- norm_gain: bfloat16 [2048], replicated, may hold values from 0.099609375 to 1.8984375
- lin_query: bfloat16 [2048, 1024], P(None, 'tp'), may hold values from -0.125 to 0.125
- lin_key: bfloat16 [2048, 1024], P(None, 'tp'), may hold values from -0.125 to 0.125
- lin_value: bfloat16 [2048, 1024], P(None, 'tp'), may hold values from -0.125 to 0.125
- lin_gate: bfloat16 [2048, 1024], P(None, 'tp'), may hold values from -0.125 to 0.125
- gate_down: bfloat16 [2048, 32], replicated, may hold values from -0.125 to 0.125
- gate_up_weight: bfloat16 [32, 1024], replicated, may hold values from -1 to 1
- decay_offset_bias: float32 [6144, 1024], P('sp', 'tp'), may hold values from -16 to 11
- lin_norm_gain: float32 [128], replicated, may hold values from 0.1 to 1.9
- stick_query: bfloat16 [2048, 1024], P(None, 'tp'), may hold values from -0.25 to 0.25
- stick_key: bfloat16 [2048, 1024], P(None, 'tp'), may hold values from -0.25 to 0.25
- stick_value: bfloat16 [2048, 1024], P(None, 'tp'), may hold values from -0.125 to 0.125
- key_bias: bfloat16 [8, 6144], P('tp', 'sp'), may hold values from -20 to -2
- out_linear: bfloat16 [1024, 2048], replicated, may hold values from -0.125 to 0.125
- out_stick: bfloat16 [1024, 2048], replicated, may hold values from -0.125 to 0.125
Outputs:
- mixed: bfloat16 [6144, 2048], P(('sp', 'tp'))
All inputs are finite; a program needn't handle non-finite values.
Results may differ from a plain program's by a relative error of at most 0.012.
Values may be sent and summed in bfloat16 or wider, within the bound.
A program may use at most 64 MiB of HBM per device.

v0:
```python
import jax
import jax.numpy as jnp
from jax import lax
from jax.sharding import Mesh
from jax.sharding import PartitionSpec as P

BLK = 32
SP = ("sp_0", "sp_1")
SP_TP = ("sp_0", "sp_1", "tp")


norm_eps = 1e-06
gate_softness = 16.0


def gather_turned(arrays, axis, dims):
    turned = [jnp.moveaxis(a, dim, 0) for a, dim in zip(arrays, dims)]
    both = jnp.concatenate([t.reshape(len(t), -1) for t in turned], axis=1)
    filled, at, outs = (lax.all_gather(both, axis, axis=0, tiled=True), 0, [])
    for t, dim in zip(turned, dims):
        share = filled[:, at : at + t[0].size].reshape(-1, *t.shape[1:])
        outs.append(jnp.moveaxis(share, 0, dim))
        at += t[0].size
    return tuple(outs)


def laid_out(parts, dim):
    lengths = list(parts.shape[1:])
    lengths[dim] *= parts.shape[0]
    return jnp.moveaxis(parts, 0, dim).reshape(lengths)


def from_everyone(array, axis):
    devices = lax.axis_size(axis)
    return lax.all_to_all(
        jnp.broadcast_to(array[None], (devices, *array.shape)), axis, 0, 0, tiled=True
    )


def collect(array, axis, dim):
    return laid_out(from_everyone(array, axis), dim)


def filled_with(array, identity):
    return jax.tree.map(
        lambda part, zero: jnp.zeros_like(part) + jnp.asarray(zero, part.dtype), array, identity
    )


def all_in_one(array, axis):
    leaves = jax.tree.leaves(array)
    turns = sorted(range(len(leaves)), key=lambda k: -leaves[k].size)
    width = (1, *leaves[turns[0]].shape)[-1]
    lines = [
        jnp.pad(leaves[k].reshape(-1), (0, -leaves[k].size % width)).reshape(-1, width)
        for k in turns
    ]
    both, at, found = (lax.all_gather(jnp.concatenate(lines), axis), 0, {})
    for k, line in zip(turns, lines):
        share = both[:, at : at + len(line)].reshape(len(both), -1)
        found[k] = share[:, : leaves[k].size].reshape(-1, *leaves[k].shape)
        at += len(line)
    numbers = iter(range(len(leaves)))
    return jax.tree.map(lambda _: found[next(numbers)], array)


def prefix_by_axis(array, axes, combine, identity):
    before = start = filled_with(array, identity)
    subtotal = array
    for axis in reversed(axes):
        devices, here = (lax.axis_size(axis), lax.axis_index(axis))
        pieces = all_in_one(
            jax.tree.map(
                lambda part, kind: part.astype(kind),
                subtotal,
                jax.tree.map(lambda a: jnp.bfloat16 if a.dtype == jnp.float32 else a.dtype, array),
            ),
            axis,
        )
        inside, subtotal = (start, start)
        for k in range(devices):
            passed = k < here
            subtotal = combine(
                subtotal, jax.tree.map(lambda part, own: part[k].astype(own.dtype), pieces, array)
            )
            inside = jax.tree.map(lambda new, old: jnp.where(passed, new, old), subtotal, inside)
        before = combine(inside, before)
    return before


def feature_fold(weights, low_weight, norm_gain, partial_value):
    gain_part = norm_gain.astype(jnp.float32)
    widened = partial_value.astype(jnp.float32)
    scaled = (widened * gain_part).astype(jnp.bfloat16)
    result = [
        jnp.dot(scaled, weights, preferred_element_type=jnp.float32),
        jnp.sum(widened * widened, axis=1),
    ]
    result.append(jnp.dot(scaled, low_weight, preferred_element_type=jnp.float32))
    return tuple(result)


def chain_states(earlier, later):
    return (earlier[0] + later[0], earlier[1] * jnp.exp(later[0])[..., None] + later[1])


def heads_first(matrix, heads):
    return matrix.reshape(matrix.shape[0], heads, -1).transpose(1, 0, 2)


def linear_local(query, keys_in, values_in, decay_logarithm, heads, block_len):
    highest_precision = lax.Precision.HIGHEST
    blocks = query.shape[0] // block_len
    head_size = query.shape[1] // heads

    def blocked(matrix):
        return matrix.reshape(blocks, block_len, heads, head_size).transpose(2, 0, 1, 3)

    queries = blocked(query).astype(jnp.float32) * head_size ** (-0.5)
    keyed = blocked(keys_in).astype(jnp.float32)
    valued = blocked(values_in)
    within_segment = jnp.cumsum(blocked(decay_logarithm), axis=2)
    causal = jnp.tril(jnp.ones((block_len, block_len), dtype=bool))
    spread = within_segment[:, :, :, None, :] - within_segment[:, :, None, :, :]
    fading = jnp.exp(jnp.where(causal[:, :, None], spread, -jnp.inf))
    scores = jnp.einsum(
        "hntd,hnsd,hntsd->hnts", queries, keyed, fading, precision=highest_precision
    ).astype(jnp.bfloat16)
    inner = jnp.einsum("hnts,hnsv->hntv", scores, valued, preferred_element_type=jnp.float32)
    last_position = within_segment[:, :, -1, :]
    weighted_keys = keyed * jnp.exp(last_position[:, :, None, :] - within_segment)
    contrib = jnp.einsum(
        "hnsd,hnsv->hndv", weighted_keys, valued.astype(jnp.float32), precision=highest_precision
    )
    totals, states = lax.associative_scan(chain_states, (last_position, contrib), axis=1)
    before = jnp.concatenate([jnp.zeros_like(states[:, :1]), states[:, :-1]], axis=1)
    offsets = jnp.concatenate([jnp.zeros_like(totals[:, :1]), totals[:, :-1]], axis=1)
    carried_state = jnp.einsum(
        "hntd,hndv->hntv", queries * jnp.exp(within_segment), before, precision=highest_precision
    )
    from_start = queries * jnp.exp(offsets[:, :, None, :] + within_segment)
    return (inner + carried_state, from_start, (totals[:, -1], states[:, -1]))


def linear_finish(local_out, from_start, incoming_state, gate_in, head_gain):
    cross = jnp.einsum(
        "hntd,hdv->hntv", from_start, incoming_state, precision=lax.Precision.HIGHEST
    )
    combined = local_out + cross
    normed = (
        combined
        * lax.rsqrt(jnp.mean(combined * combined, axis=-1, keepdims=True) + norm_eps)
        * head_gain
    )
    token_major = normed.transpose(1, 2, 0, 3).reshape(gate_in.shape)
    return (token_major * jax.nn.silu(gate_in.astype(jnp.float32))).astype(jnp.bfloat16)


def later_sums(falling):
    heads, rows, keys_count = falling.shape
    piece = min(128, keys_count)
    pieces = keys_count // piece
    grouped = falling.reshape(heads, rows, pieces, piece)
    inner_index = jnp.arange(piece, dtype=jnp.int32)
    strict_inner = (inner_index[:, None] > inner_index[None, :]).astype(jnp.float32)
    within = jnp.einsum("htnj,js->htns", grouped, strict_inner, precision=lax.Precision.HIGHEST)
    piece_index = jnp.arange(pieces, dtype=jnp.int32)
    strict_outer = (piece_index[:, None] > piece_index[None, :]).astype(jnp.float32)
    after = jnp.einsum(
        "htm,mn->htn", jnp.sum(grouped, axis=3), strict_outer, precision=lax.Precision.HIGHEST
    )
    return (within + after[..., None]).reshape(heads, rows, keys_count)


def stick_block(running, queries, keys_in, values_in, bias_in, visible):
    weighted, consumed = running
    head_size = queries.shape[-1]
    logits = jnp.einsum(
        "htd,hsd->hts", queries, keys_in, preferred_element_type=jnp.float32
    ) * head_size ** (-0.5)
    logits = logits + bias_in.astype(jnp.float32)[:, None, :]
    falling = jnp.where(visible, jax.nn.log_sigmoid(-logits), 0.0)
    behind = later_sums(falling)
    shares = jnp.where(
        visible, jnp.exp(jax.nn.log_sigmoid(logits) + behind + consumed[:, :, None]), 0.0
    ).astype(jnp.bfloat16)
    weighted = weighted + jnp.einsum(
        "hts,hsd->htd", shares, values_in, preferred_element_type=jnp.float32
    )
    return (weighted, consumed + jnp.sum(falling, axis=2))


def collect_keys(packed, key_bias):
    return gather_turned((packed, key_bias), SP, (2, 1))


def per_device(
    tokens,
    norm_gain,
    lin_query,
    lin_key,
    lin_value,
    lin_gate,
    gate_down,
    gate_up_weight,
    decay_offset_bias,
    lin_norm_gain,
    stick_query,
    stick_key,
    stick_value,
    key_bias,
    out_linear,
    out_stick,
):
    model_width = norm_gain.shape[0]
    head_size = lin_norm_gain.shape[0]
    token_count = tokens.shape[0]
    lin_cols = lin_query.shape[1]
    stick_cols = stick_query.shape[1]
    lin_heads = lin_cols // head_size
    stick_heads = stick_cols // head_size
    lin_weights = [lin_query, lin_key, lin_value, lin_gate]
    stick_weights = [stick_query, stick_key, stick_value]
    all_joined = jnp.concatenate(lin_weights + stick_weights, axis=1)
    both_acc, squares, low_acc = feature_fold(
        all_joined, gate_down, norm_gain, collect(tokens, "tp", 1)
    )
    lin_acc = both_acc[:, : 4 * lin_cols]
    stick_acc = both_acc[:, 4 * lin_cols :]
    rescale = lax.rsqrt(squares / model_width + norm_eps)[:, None]
    lin_proj = (lin_acc * rescale).astype(jnp.bfloat16)
    stick_proj = (stick_acc * rescale).astype(jnp.bfloat16)
    reduced_rank = (low_acc * rescale).astype(jnp.bfloat16)
    up_cols = lax.dynamic_slice_in_dim(gate_up_weight, lax.axis_index("tp") * lin_cols, lin_cols, 1)
    decay_logarithm = (
        jax.nn.log_sigmoid(
            jnp.dot(reduced_rank, up_cols, preferred_element_type=jnp.float32) + decay_offset_bias
        )
        / gate_softness
    )
    local_out, from_start, summary = linear_local(
        lin_proj[:, :lin_cols],
        lin_proj[:, lin_cols : 2 * lin_cols],
        lin_proj[:, 2 * lin_cols : 3 * lin_cols],
        decay_logarithm,
        lin_heads,
        BLK,
    )
    identity = (jnp.zeros_like(summary[0]), jnp.zeros_like(summary[1]))
    incoming = prefix_by_axis(summary, SP, chain_states, identity)
    linear_out = linear_finish(
        local_out, from_start, incoming[1], lin_proj[:, 3 * lin_cols :], lin_norm_gain
    )
    stick_q = heads_first(stick_proj[:, :stick_cols], stick_heads)
    stick_k = heads_first(stick_proj[:, stick_cols : 2 * stick_cols], stick_heads)
    stick_v = heads_first(stick_proj[:, 2 * stick_cols :], stick_heads)
    own_mask = jnp.tril(jnp.ones((token_count, token_count), dtype=bool), -1)
    position = lax.axis_index(SP)
    packed = jnp.stack([stick_k, stick_v])
    start_state = (
        jnp.zeros((stick_heads, token_count, head_size), jnp.float32),
        jnp.zeros((stick_heads, token_count), jnp.float32),
    )
    running = stick_block(start_state, stick_q, stick_k, stick_v, key_bias, own_mask)
    every_pair, every_bias = collect_keys(packed, key_bias)

    def visit_all(distance, running_in):
        source = (position - distance) * token_count
        pair_part = lax.dynamic_slice_in_dim(every_pair, source, token_count, 2)
        bias_part = lax.dynamic_slice_in_dim(every_bias, source, token_count, 1)
        return stick_block(running_in, stick_q, pair_part[0], pair_part[1], bias_part, True)

    running = lax.fori_loop(1, position + 1, visit_all, running)
    stick_heads_out = running[0].astype(jnp.bfloat16)
    stick_out = stick_heads_out.transpose(1, 0, 2).reshape(token_count, stick_cols)
    tp_span = lax.axis_size("tp")
    joined_cols = lin_cols + stick_cols
    merged = jnp.concatenate([linear_out, stick_out], axis=1).reshape(
        tp_span, token_count // tp_span, joined_cols
    )
    received = lax.all_to_all(merged, "tp", split_axis=0, concat_axis=2, tiled=True)
    row_count = received.shape[1]
    parts = received.reshape(row_count, tp_span, joined_cols)
    lin_part = parts[:, :, :lin_cols].reshape(row_count, tp_span * lin_cols)
    stick_part = parts[:, :, lin_cols:].reshape(row_count, tp_span * stick_cols)
    total = jnp.dot(lin_part, out_linear, preferred_element_type=jnp.float32) + jnp.dot(
        stick_part, out_stick, preferred_element_type=jnp.float32
    )
    result = total.astype(jnp.bfloat16)[None]
    return result[0]


def solution(mesh):
    torus = Mesh(mesh.devices.reshape(4, 4, mesh.shape["tp"]), ("sp_0", "sp_1", "tp"))
    placed = (
        P(SP, "tp"),
        P(),
        P(None, "tp"),
        P(None, "tp"),
        P(None, "tp"),
        P(None, "tp"),
        P(),
        P(),
        P(SP, "tp"),
        P(),
        P(None, "tp"),
        P(None, "tp"),
        P(None, "tp"),
        P("tp", SP),
        P(),
        P(),
    )
    return jax.shard_map(
        per_device, mesh=torus, in_specs=placed, out_specs=P(SP_TP, None), check_vma=False
    )
```

profile of v0, /device:TPU:102, one launch (start us, length us, event | category | flops | bytes accessed | tf_op | source)
XLA Modules:
  0.0 180.7 jit_solution(1187905086112378748)
XLA Ops:
  9.1 4.5 %all-to-all-start = ((bf16[8,384,256]{1,2,0:T(8,128)(2,1)}), bf16[8,384,256]{1,2,0:T(8,128)(2,1)S(1)}, u32[]{:S(2)}, u32[]{:S(2)}) async-start(bf16[8,384,256]{1,2,0:T(8,128)(2,1)} %broadcast_in_dim.28), calls=%async_computation | async-start | bytes 3145728 | tf_op jit(solution)/shard_map/all_to_all | solution.py:35
  16.4 1.9 %constant_dynamic-update-slice_fusion.3 = bf16[2048,896]{1,0:T(8,128)(2,1)} fusion(bf16[2048,896]{1,0:T(8,128)(2,1)} %constant_dynamic-update-slice_fusion.4, bf16[2048,128]{1,0:T(8,128)(2,1)} %param.23), kind=kLoop, calls=%fused_computation.184 | loop fusion | bytes 1048576
  18.3 1.9 %constant_dynamic-update-slice_fusion.2 = bf16[2048,896]{1,0:T(8,128)(2,1)} fusion(bf16[2048,896]{1,0:T(8,128)(2,1)} %constant_dynamic-update-slice_fusion.3, bf16[2048,128]{1,0:T(8,128)(2,1)} %param.28), kind=kLoop, calls=%fused_computation.183 | loop fusion | bytes 1048576
  22.0 13.1 %all-to-all-done = bf16[8,384,256]{1,2,0:T(8,128)(2,1)S(1)} async-done(((bf16[8,384,256]{1,2,0:T(8,128)(2,1)}), bf16[8,384,256]{1,2,0:T(8,128)(2,1)S(1)}, u32[]{:S(2)}, u32[]{:S(2)}) %all-to-all-start) | async-done | bytes 1572896 | tf_op jit(solution)/shard_map/all_to_all | solution.py:35
  39.0 3.8 %fusion.141 = f32[384,896]{1,0:T(8,128)S(1)} fusion(bf16[384,2048]{0,1:T(8,128)(2,1)S(1)} %fusion.17, bf16[2048,896]{1,0:T(8,128)(2,1)} %constant_dynamic-update-slice_fusion), kind=kOutput, calls=%fused_computation.254 | convolution fusion | flops 1409286144 | bytes 6619136 | tf_op jit(solution)/shard_map/dot_general | solution.py:96
  46.7 2.8 %pad.112 = f32[1,11,128,128]{3,2,1,0:T(8,128)} pad(f32[1,6,128,128]{3,2,1,0:T(8,128)S(1)} %add.381, f32[]{:T(128)} %constant.24.clone.1), padding=0_0_0x0_0_1x0_0_0x0_0_0 | pad | bytes 1114116
  49.7 1.7 fusion.44
  54.2 4.9 %fusion.16 = bf16[12,32,32]{1,2,0:T(8,128)(2,1)S(1)} fusion(f32[12,32,32,128]{3,2,1,0:T(8,128)S(1)} %select_exponential_fusion, f32[12,128,32]{1,2,0:T(8,128)S(1)} %bitcast.216, f32[12,128,32]{1,2,0:T(8,128)S(1)} %convert_bitcast_fusion), kind=kLoop, calls=%fused_computation.27 | loop fusion | flops 4706304 | bytes 6709248
  60.7 12.1 %all-gather.2 = bf16[4,129,128]{2,1,0:T(8,128)(2,1)S(1)} all-gather(bf16[1,129,128]{2,1,0:T(8,128)(2,1)S(1)} %maximum_bitcast_fusion.1), channel_id=2, replica_groups=mesh['sp_0'=4,'sp_1'=4,'tp'=8] {'sp_1'}, dimensions={0}, use_global_device_ids=true | all-gather | bytes 165120 | tf_op jit(solution)/shard_map/all_gather | solution.py:58
  73.1 12.5 %all-gather.3 = bf16[4,129,128]{2,1,0:T(8,128)(2,1)S(1)} all-gather(bf16[1,129,128]{2,1,0:T(8,128)(2,1)S(1)} %maximum_bitcast_fusion.2), channel_id=3, replica_groups=mesh['sp_0'=4,'sp_1'=4,'tp'=8] {'sp_0'}, dimensions={0}, use_global_device_ids=true | all-gather | bytes 165120 | tf_op jit(solution)/shard_map/all_gather | solution.py:58
  86.2 1.6 fusion.30
  90.9 4.5 %all-gather.6.cloned.1.call-done = bf16[6144,257]{0,1:T(8,128)(2,1)} async-done(((bf16[384,257]{0,1:T(8,128)(2,1)}), bf16[6144,257]{0,1:T(8,128)(2,1)}) %all-gather.6.cloned.1.call-update) | async-done | bytes 3158032 | tf_op jit(solution)/shard_map/all_gather | solution.py:19
  96.3 3.9 %slice.324 = bf16[6144,256]{0,1:T(8,128)(2,1)} slice(bf16[6144,257]{0,1:T(8,128)(2,1)} %all-gather.6.cloned.1.call-done), slice={[0:6144], [0:256]} | slice | bytes 6291456 | tf_op jit(solution)/shard_map/slice | solution.py:21
  100.2 58.5 %while.12 = (s32[]{:T(128)}, f32[1,384,128]{2,1,0:T(8,128)S(1)}, f32[1,384]{1,0:T(1,128)S(1)}, s32[]{:T(128)}, s32[]{:T(128)}, /*index=5*/bf16[2,1,6144,128]{2,3...) while((s32[]{:T(128)}, f32[1,384,128]{2,1,0:T(8,128)S(1)}, ...), condition=%wide.region_8.9_spmd, body=%wide.region_5.8_spmd.sunk | while | flops 305488000 | bytes 5441511 | solution.py:273
  100.2 1.5 fusion.170
  104.1 1.5 fusion.170
  108.0 1.5 fusion.170
  111.9 1.5 fusion.170
  115.8 1.5 fusion.170
  119.7 1.5 fusion.170
  123.6 1.5 fusion.170
  127.5 1.5 fusion.170
  131.4 1.5 fusion.170
  135.3 1.5 fusion.170
  139.2 1.5 fusion.170
  143.1 1.5 fusion.170
  147.0 1.5 fusion.170
  150.9 1.5 fusion.170
  154.8 1.5 fusion.170
  158.7 10.5 %all_to_all.20 = bf16[8,48,256]{2,1,0:T(8,128)(2,1)S(1)} all-to-all(bf16[8,48,256]{2,1,0:T(8,128)(2,1)S(1)} %pad_maximum_fusion.3), channel_id=1, replica_groups=mesh['sp_0'=4,'sp_1'=4,'tp'=8] {'tp'}, dimensions={0} | all-to-all | bytes 393216 | tf_op jit(solution)/shard_map/all_to_all | solution.py:281
  169.3 3.0 %fusion.55 = f32[48,2048]{1,0:T(8,128)S(1)} fusion(bf16[1024,2048]{1,0:T(8,128)(2,1)} %param.32, bf16[8,6,8,128]{3,2,1,0:T(8,128)(2,1)S(1)} %get-tuple-element.118), kind=kOutput, calls=%fused_computation.104 | convolution fusion | flops 201326592 | bytes 4685824 | tf_op jit(solution)/shard_map/dot_general | solution.py:286
  172.3 1.5 fusion.18
  (259 shorter events, 59.3 us)
Async XLA Ops:
  6.5 29.3 %copy-start = (bf16[2048,32]{0,1:T(8,128)(2,1)S(1)}, bf16[2048,32]{0,1:T(8,128)(2,1)}, u32[]{:S(2)}) copy-start(bf16[2048,32]{0,1:T(8,128)(2,1)} %param.24) | copy-start | bytes 393220
  6.5 7.1 %copy-start.17 = (bf16[1,384]{1,0:T(2,128)(2,1)S(1)}, bf16[1,384]{1,0:T(2,128)(2,1)}, u32[]{:S(2)}) copy-start(bf16[1,384]{1,0:T(2,128)(2,1)} %param.31) | copy-start | bytes 2308
  6.5 7.1 %copy-start.18 = (bf16[2048]{0:T(1024)(128)(2,1)S(1)}, bf16[2048]{0:T(1024)(128)(2,1)}, u32[]{:S(2)}) copy-start(bf16[2048]{0:T(1024)(128)(2,1)} %param.19) | copy-start | bytes 12292
  6.5 7.1 %copy-start.9 = (bf16[2048,128]{1,0:T(8,128)(2,1)S(1)}, bf16[2048,128]{1,0:T(8,128)(2,1)}, u32[]{:S(2)}) copy-start(bf16[2048,128]{1,0:T(8,128)(2,1)} %param.20) | copy-start | bytes 1572868
  6.5 8.0 %copy-start.10 = (bf16[2048,128]{1,0:T(8,128)(2,1)S(1)}, bf16[2048,128]{1,0:T(8,128)(2,1)}, u32[]{:S(2)}) copy-start(bf16[2048,128]{1,0:T(8,128)(2,1)} %param.21) | copy-start | bytes 1572868
  6.5 8.9 %copy-start.11 = (bf16[2048,128]{1,0:T(8,128)(2,1)S(1)}, bf16[2048,128]{1,0:T(8,128)(2,1)}, u32[]{:S(2)}) copy-start(bf16[2048,128]{1,0:T(8,128)(2,1)} %param.22) | copy-start | bytes 1572868
  9.1 26.0 %all-to-all-start = ((bf16[8,384,256]{1,2,0:T(8,128)(2,1)}), bf16[8,384,256]{1,2,0:T(8,128)(2,1)S(1)}, u32[]{:S(2)}, u32[]{:S(2)}) async-start(bf16[8,384,256]{1,2,0:T(8,128)(2,1)} %broadcast_in_dim.28), calls=%async_computation | async-start | bytes 3145728 | tf_op jit(solution)/shard_map/all_to_all | solution.py:35
  13.5 81.9 %all-gather.6.cloned.1.call-start = ((), (), s32[]{:S(2)}) async-start(), calls=%async_computation.2 | async-start | bytes 3446784 | tf_op jit(solution)/shard_map/all_gather | solution.py:19
  14.6 5.7 %copy-start.12 = (bf16[2048,128]{1,0:T(8,128)(2,1)S(1)}, bf16[2048,128]{1,0:T(8,128)(2,1)}, u32[]{:S(2)}) copy-start(bf16[2048,128]{1,0:T(8,128)(2,1)} %param.29) | copy-start | bytes 1572868
  14.6 6.5 %copy-start.13 = (bf16[2048,128]{1,0:T(8,128)(2,1)S(1)}, bf16[2048,128]{1,0:T(8,128)(2,1)}, u32[]{:S(2)}) copy-start(bf16[2048,128]{1,0:T(8,128)(2,1)} %param.30) | copy-start | bytes 1572868
  20.2 15.6 %copy-start.15 = (f32[384,128]{1,0:T(8,128)S(1)}, f32[384,128]{1,0:T(8,128)}, u32[]{:S(2)}) copy-start(f32[384,128]{1,0:T(8,128)} %param.26) | copy-start | bytes 589828
  42.9 2.8 %copy-start.2 = (bf16[384,384]{1,0:T(8,128)(2,1)}, bf16[384,384]{1,0:T(8,128)(2,1)S(1)}, u32[]{:S(2)}) copy-start(bf16[384,384]{1,0:T(8,128)(2,1)S(1)} %fusion.33) | copy-start | bytes 884740
  43.1 2.7 %copy-start.4 = (bf16[384,512]{1,0:T(8,128)(2,1)}, bf16[384,512]{1,0:T(8,128)(2,1)S(1)}, u32[]{:S(2)}) copy-start(bf16[384,512]{1,0:T(8,128)(2,1)S(1)} %fusion.22) | copy-start | bytes 1179652
  43.1 3.4 %copy-start.5 = (bf16[384,128]{1,0:T(8,128)(2,1)}, bf16[384,128]{1,0:T(8,128)(2,1)S(1)}, u32[]{:S(2)}) copy-start(bf16[384,128]{1,0:T(8,128)(2,1)S(1)} %get-tuple-element.111) | copy-start | bytes 294916
  43.1 3.4 %copy-start.7 = (bf16[384,128]{1,0:T(8,128)(2,1)}, bf16[384,128]{1,0:T(8,128)(2,1)S(1)}, u32[]{:S(2)}) copy-start(bf16[384,128]{1,0:T(8,128)(2,1)S(1)} %get-tuple-element.110) | copy-start | bytes 294916
  49.7 2.0 %copy-start.3 = (bf16[384,384]{1,0:T(8,128)(2,1)S(1)}, bf16[384,384]{1,0:T(8,128)(2,1)}, u32[]{:S(2)}) copy-start(bf16[384,384]{1,0:T(8,128)(2,1)} %copy-done.2) | copy-start | bytes 884740
  49.7 3.4 %copy-start.8 = (bf16[384,128]{1,0:T(8,128)(2,1)S(1)}, bf16[384,128]{1,0:T(8,128)(2,1)}, u32[]{:S(2)}) copy-start(bf16[384,128]{1,0:T(8,128)(2,1)} %copy-done.7) | copy-start | bytes 294916
  60.7 28.2 %copy-start.6 = (bf16[384,128]{1,0:T(8,128)(2,1)S(1)}, bf16[384,128]{1,0:T(8,128)(2,1)}, u32[]{:S(2)}) copy-start(bf16[384,128]{1,0:T(8,128)(2,1)} %copy-done.5) | copy-start | bytes 294916
  85.7 3.4 %copy-start.14 = (f32[384,128]{1,0:T(8,128)S(1)}, f32[384,128]{1,0:T(8,128)}, u32[]{:S(2)}) copy-start(f32[384,128]{1,0:T(8,128)} %get-tuple-element.108) | copy-start | bytes 589828
  86.2 3.6 %copy-start.19 = (f32[128]{0:T(128)S(1)}, f32[128]{0:T(128)}, u32[]{:S(2)}) copy-start(f32[128]{0:T(128)} %param.27) | copy-start | bytes 1540
  89.7 10.5 %copy-start.16 = (bf16[1,384,128]{2,1,0:T(8,128)(2,1)S(1)}, bf16[1,384,128]{2,1,0:T(8,128)(2,1)}, u32[]{:S(2)}) copy-start(bf16[1,384,128]{2,1,0:T(8,128)(2,1)} %get-tuple-element.210) | copy-start | bytes 294916
  158.7 13.7 %copy-start.1 = (bf16[1024,2048]{1,0:T(8,128)(2,1)S(1)}, bf16[1024,2048]{1,0:T(8,128)(2,1)}, u32[]{:S(2)}) copy-start(bf16[1024,2048]{1,0:T(8,128)(2,1)} %param.33) | copy-start | bytes 12582916
Sparse Core Ops, SparseCore 0:
  45.0 50.3 all-gather.5
where the time goes:
time: 182 us; the launch traced here: 181 us
  matrix products  63.8 us (35%)
  blocking collectives  35.1 us (19%)
  other arithmetic  23.1 us (13%)
  local copies, waits for them, and re-layouts  21.6 us (12%)
  waiting for transfers between devices  17.6 us (10%)
  between operations  14.1 us (8%)
  starting transfers between devices  4.51 us (2%)
    all_gather x2, blocking collectives, all_in_one(): both, at, found = (lax.all_gather(jnp.concatenate(lines), axis), 0, {})  24.6 us
    dot_general x16, matrix products, stick_block(): jnp.einsum('htd,hsd->hts', queries, keys_in, preferred_element_type=jnp.f...  23.5 us
    dot_general x16, matrix products, stick_block(): jnp.einsum('hts,hsd->htd', shares, values_in, preferred_element_type=jnp....  18 us
    all_to_all x1, waiting for transfers between devices, from_everyone(): lax.all_to_all(jnp.broadcast_to(array[None], (devices, *array.shape)), ax...  13.1 us
    unnamed x50, local copies, waits for them, and re-layouts  12.7 us
    all_to_all x1, blocking collectives, per_device(): lax.all_to_all(merged, 'tp', split_axis=0, concat_axis=2, tiled=True)  10.5 us
    convert_element_type x16, other arithmetic, stick_block(): shares = jnp.where(visible, jnp.exp(jax.nn.log_sigmoid(logits) + behind +...  8.3 us
    dot_general x16, matrix products, later_sums(): jnp.einsum('htnj,js->htns', grouped, strict_inner, precision=lax.Precisio...  7.09 us
  transfers between devices with their start and end apart: 2, of which 2 were waited for; matrix products, arithmetic and copies ran while one was open for 16% of the time, Pallas kernels for 0%

commit v1 on v0

v1 whole, which is shorter than its diff:
```python
import jax
import jax.numpy as jnp
from jax import lax
from jax.experimental import pallas as pl
from jax.experimental.pallas import tpu as pltpu
from jax.sharding import Mesh
from jax.sharding import PartitionSpec as P

MESH = pl.DeviceIdType.MESH
F32 = jnp.float32
BF16 = jnp.bfloat16
LOG2E = 1.4426950408889634
EPS = 1e-6
SOFT = 16.0
TOK = 384
D = 2048
HD = 128
PARTS = 3
ROWS = TOK // PARTS
CH = TOK // 128
LEVELS = 7
OUT_ROWS = TOK // 8

M_A, M_B, M_P0, M_C, M_D, M_P1, M_P2, M_P3, M_P4 = [PARTS * i for i in range(9)]
M_K = 9 * PARTS
M_SX = M_K + 6
M_Q = M_SX + 4
M_SZ = M_Q + 4
M_PO = M_SZ + 4
M_LA = M_PO + 4
M_ST = M_LA + 8
N_MSG = M_ST + 8


def nt(a, b):
    return lax.dot_general(a, b, (((1,), (1,)), ((), ())), preferred_element_type=F32)


def tn(a, b):
    return lax.dot_general(a, b, (((0,), (0,)), ((), ())), preferred_element_type=F32)


def mm(a, b):
    return jnp.dot(a, b, preferred_element_type=F32)


def iota(shape, dim):
    return lax.broadcasted_iota(jnp.int32, shape, dim)


def split(x):
    hi = x.astype(BF16)
    return hi, (x - hi.astype(F32)).astype(BF16)


def rows_of(pieces):
    io = iota((16, 128), 0)
    out = jnp.zeros((16, 128), F32)
    for r, piece in enumerate(pieces):
        out = jnp.where(io == r, piece.astype(F32), out)
    return out.astype(BF16)


def kernel(
    tokens, gain, w_lq, w_lk, w_lv, w_lg, w_gd, w_gu, dob, lgain, w_sq, w_sk, w_sv, kbias, w_ol, w_os,
    out,
    tok, wbuf, gd, gu, gf, acc, ss, dbuf, kb, lng, ol, os_,
    mcon, tri, kbuf, vbuf, qbuf, lq, lk, lv, lg, lacc, qx, sx, sz, pbuf, tbuf, sbuf, rbuf, stk, ctot,
    linb, stb, xl, xs, oacc,
    lsem, ssem, rsem,
):
    a, b = lax.axis_index("z"), lax.axis_index("x")
    y, c = lax.axis_index("y"), lax.axis_index("c")
    tp = 2 * y + c
    oc = 1 - c

    def local(src, dst, i):
        cp = pltpu.make_async_copy(src, dst, lsem.at[i])
        cp.start()
        return cp

    def remote(src, dst, i, **dev):
        return pltpu.make_async_remote_copy(
            src_ref=src, dst_ref=dst, send_sem=ssem.at[i], recv_sem=rsem.at[i],
            device_id=dev, device_id_type=MESH,
        )

    def arrived(dst, i):
        remote(dst, dst, i, c=oc).wait_recv()

    def sent(src, i):
        remote(src, src, i, c=oc).wait_send()

    base = 4 * y + 2 * c
    loads = [
        local(tokens.at[:, pl.ds(0, 128)], tok.at[base], 0),
        local(tokens.at[:, pl.ds(128, 128)], tok.at[base + 1], 1),
    ]
    weights = [w_sk, w_sv, w_sq, w_lk, w_lv, w_lq, w_lg]
    wloads = [local(w, wbuf.at[:, pl.ds(128 * i, 128)], 2 + i) for i, w in enumerate(weights)]
    gdl = local(w_gd, gd, 9)
    gainl = local(gain, gf, 10)
    kbl = local(kbias, kb, 11)
    gul = local(w_gu.at[:, pl.ds(pl.multiple_of(128 * tp, 128), 128)], gu, 12)
    dobl = local(dob, dbuf, 13)
    lngl = local(lgain, lng, 14)
    oll = local(w_ol, ol, 15)
    osl = local(w_os, os_, 16)

    barrier = pltpu.get_barrier_semaphore()
    for k in range(1, 4):
        pl.semaphore_signal(barrier, inc=1, device_id={"x": lax.rem(b + k, 4)}, device_id_type=MESH)
        pl.semaphore_signal(barrier, inc=1, device_id={"z": lax.rem(a + k, 4)}, device_id_type=MESH)
    for k in range(1, 8):
        r = lax.rem(tp + k, 8)
        pl.semaphore_signal(
            barrier, inc=1, device_id={"y": r // 2, "c": lax.rem(r, 2)}, device_id_type=MESH
        )

    t_i, s_i = iota((128, 128), 0), iota((128, 128), 1)
    for lev in range(LEVELS):
        same = (t_i >> lev) == (s_i >> lev)
        second = ((t_i >> lev) & 1) == 1
        m = jnp.where(same, jnp.where(second, jnp.where(s_i <= t_i, 1.0, 0.0), jnp.where(s_i > t_i, 1.0, 0.0)), 0.0)
        mcon[pl.ds(128 * lev, 128), :] = m.astype(BF16)
    mcon[pl.ds(128 * LEVELS, 128), :] = jnp.where(s_i <= t_i, 1.0, 0.0).astype(BF16)
    mcon[pl.ds(128 * LEVELS + 128, 128), :] = jnp.where(s_i > t_i, 1.0, 0.0).astype(BF16)
    tri[...] = jnp.where(iota((256, 256), 0) > iota((256, 256), 1), 1.0, 0.0).astype(BF16)
    for g in range(4):
        pbuf[g, 0] = jnp.zeros((TOK, HD), F32)
        tbuf[g, 0] = jnp.zeros((TOK, HD), F32)

    for cp in loads:
        cp.wait()
    pl.semaphore_wait(barrier, 13)

    yp, ym, yo = lax.rem(y + 1, 4), lax.rem(y + 3, 4), lax.rem(y + 2, 4)

    def part(first, count, r):
        return tok.at[pl.ds(first, count), pl.ds(ROWS * r, ROWS), :]

    started = []

    def send(src, dst, i, **dev):
        remote(src, dst, i, **dev).start()
        started.append((src, i))

    for r in range(PARTS):
        mine = part(base, 2, r)
        send(mine, mine, M_A + r, y=yp)
        send(mine, mine, M_B + r, y=ym)
        send(mine, mine, M_P0 + r, c=oc)

    gainl.wait()
    kbl.wait()
    kbuf[b, pl.ds(TOK, 16), :] = rows_of([kb[:, pl.ds(128 * r, 128)] for r in range(CH)])
    for cp in wloads:
        cp.wait()
    gdl.wait()
    wbuf[:, pl.ds(896, 128)] = jnp.zeros((D, 128), BF16)
    wbuf[:, pl.ds(896, 32)] = gd[...]

    def scaled(chip, first=False):
        pieces = []
        for j in range(4):
            x = tok[4 * chip + j].astype(F32)
            sq = x * x
            ss[...] = sq if (first and j == 0) else ss[...] + sq
            pieces.append((x * gf[pl.ds(4 * chip + j, 1), :]).astype(BF16))
        return jnp.concatenate(pieces, axis=1)

    def weight_rows(chip):
        return pl.ds(pl.multiple_of(512 * chip, 512), 512)

    def fold(chip, first=False):
        lhs = scaled(chip, first)
        for n in range(4):
            cols = pl.ds(256 * n, 256)
            add = mm(lhs, wbuf[weight_rows(chip), cols])
            acc[:, cols] = add if first else acc[:, cols] + add

    for r in range(PARTS):
        arrived(part(4 * y + 2 * oc, 2, r), M_P0 + r)
    fold(y, True)
    for r in range(PARTS):
        arrived(part(4 * ym + 2 * c, 2, r), M_A + r)
        one = part(4 * ym + 2 * c, 1, r)
        send(one, one, M_C + r, y=yp)
        both = part(4 * ym + 2 * c, 2, r)
        send(both, both, M_P1 + r, c=oc)
        arrived(part(4 * yp + 2 * c, 2, r), M_B + r)
        one = part(4 * yp + 2 * c + 1, 1, r)
        send(one, one, M_D + r, y=ym)
        both = part(4 * yp + 2 * c, 2, r)
        send(both, both, M_P2 + r, c=oc)
    for r in range(PARTS):
        arrived(part(4 * ym + 2 * oc, 2, r), M_P1 + r)
    fold(ym)
    for r in range(PARTS):
        arrived(part(4 * yp + 2 * oc, 2, r), M_P2 + r)
    fold(yp)
    for r in range(PARTS):
        one = part(4 * yo + 2 * c, 1, r)
        arrived(one, M_C + r)
        send(one, one, M_P3 + r, c=oc)
        one = part(4 * yo + 2 * c + 1, 1, r)
        arrived(one, M_D + r)
        send(one, one, M_P4 + r, c=oc)
    for r in range(PARTS):
        arrived(part(4 * yo + 2 * oc, 1, r), M_P3 + r)
        arrived(part(4 * yo + 2 * oc + 1, 1, r), M_P4 + r)

    lhs = scaled(yo)
    inv = lax.rsqrt(jnp.sum(ss[...], axis=1, keepdims=True) * (1.0 / D) + EPS)

    def finish(n):
        cols = pl.ds(256 * n, 256)
        total = acc[:, cols] + mm(lhs, wbuf[weight_rows(yo), cols])
        return (total * inv).astype(BF16)

    xp, xm, xo = lax.rem(b + 1, 4), lax.rem(b + 3, 4), lax.rem(b + 2, 4)
    got = finish(0)
    kbuf[b, pl.ds(0, TOK), :] = got[:, :128]
    vbuf[b] = got[:, 128:]
    send(kbuf.at[b], kbuf.at[b], M_K, x=xp)
    send(kbuf.at[b], kbuf.at[b], M_K + 1, x=xm)
    send(vbuf.at[b], vbuf.at[b], M_K + 2, x=xp)
    send(vbuf.at[b], vbuf.at[b], M_K + 3, x=xm)
    got = finish(1)
    qbuf[0] = got[:, :128]
    lk[...] = got[:, 128:]
    for d in range(1, 4):

        @pl.when(a >= d)
        def _():
            remote(qbuf.at[0], qbuf.at[d], M_Q + d, z=a - d).start()

    got = finish(2)
    lv[...] = got[:, :128]
    lq[...] = got[:, 128:]
    got = finish(3)
    lg[...] = got[:, :128]
    low = got[:, 128:160]

    gul.wait()
    dobl.wait()
    pre = (mm(low, gu[...]) + dbuf[...]) * LOG2E
    decay = (jnp.minimum(pre, 0.0) - jnp.log2(1.0 + jnp.exp2(-jnp.abs(pre)))) * (1.0 / SOFT)
    ghi, glo = split(decay)
    gboth = jnp.concatenate([ghi, glo], axis=1)
    scale = HD ** (-0.5)
    apart = t_i ^ s_i
    state = jnp.zeros((HD, HD), F32)
    before = jnp.zeros((1, HD), F32)
    for n in range(CH):
        rows = slice(128 * n, 128 * n + 128)
        both = mm(mcon[...], gboth[rows])
        dist = both[:, :128] + both[:, 128:]
        fade = jnp.exp2(dist)
        qh, kh, vh = lq[rows, :], lk[rows, :], lv[rows, :]
        qf, kf = qh.astype(F32) * scale, kh.astype(F32)
        score = jnp.where(apart == 0, nt(qh, kh) * scale, 0.0)
        for lev in range(LEVELS):
            e = fade[128 * lev : 128 * lev + 128]
            part_score = nt((qf * e).astype(BF16), (kf * e).astype(BF16))
            score = jnp.where(((apart >> lev) == 1) & (t_i > s_i), part_score, score)
        inner = mm(score.astype(BF16), vh)
        from_start = fade[128 * LEVELS : 128 * LEVELS + 128]
        to_end = fade[128 * LEVELS + 128 :]
        qs = qf * from_start
        if n:
            inner = inner + nt(qs.astype(BF16), state.astype(BF16))
        lacc[rows, :] = inner
        qx[rows, :] = (qs * jnp.exp2(before)).astype(BF16)
        length = dist[128 * LEVELS + 127 : 128 * LEVELS + 128]
        state = state * jnp.exp2(length) + tn(vh, (kf * to_end).astype(BF16))
        before = before + length
    sx[b, pl.ds(0, HD), :] = state.astype(BF16)
    sx[b, pl.ds(HD, 16), :] = rows_of(split(before))
    for k in range(1, 4):
        send(sx.at[b], sx.at[b], M_SX + k, x=lax.rem(b + k, 4))

    def pair(d, g, diagonal):
        head = kbuf[g, pl.ds(TOK, 16), :].astype(F32) * LOG2E
        bias = jnp.concatenate([head[r : r + 1] for r in range(CH)], axis=1)
        z = nt(qbuf[d], kbuf[g, pl.ds(0, TOK), :]) * (scale * LOG2E) + bias
        soft = jnp.maximum(z, 0.0) + jnp.log2(1.0 + jnp.exp2(-jnp.abs(z)))
        own = z - soft
        if diagonal:
            seen = iota((TOK, TOK), 1) < iota((TOK, TOK), 0)
            soft = jnp.where(seen, soft, 0.0)
        sb = soft.astype(BF16)
        near = mm(sb[:, 256:], tri[pl.ds(0, 128), pl.ds(0, 128)])
        near_total = near[:, :1] + soft[:, 256:257]
        far = mm(sb[:, :256], tri[...]) + near_total
        whole = far[:, :1] + soft[:, :1]
        share = jnp.exp2(own - jnp.concatenate([far, near], axis=1))
        if diagonal:
            share = jnp.where(seen, share, 0.0)
        pbuf[g, d] = mm(share.astype(BF16), vbuf[g])
        tbuf[g, d] = jnp.broadcast_to(whole, (TOK, HD))

    def pairs(g, first):
        def body(d, carry):
            pair(d, g, False)
            return carry

        lax.fori_loop(first, 4 - a, body, 0)

    pair(0, b, True)
    for d in range(1, 4):

        @pl.when(a + d <= 3)
        def _():
            arrived(qbuf.at[d], M_Q + d)

    pairs(b, 1)
    arrived(kbuf.at[xm], M_K)
    send(kbuf.at[xm], kbuf.at[xm], M_K + 4, x=xp)
    arrived(kbuf.at[xp], M_K + 1)
    arrived(vbuf.at[xp], M_K + 3)
    send(vbuf.at[xp], vbuf.at[xp], M_K + 5, x=xm)
    arrived(vbuf.at[xm], M_K + 2)
    pairs(xm, jnp.where(xm < b, 0, 1))
    pairs(xp, jnp.where(xp < b, 0, 1))

    for k in range(1, 4):
        arrived(sx.at[lax.rem(b + 4 - k, 4)], M_SX + k)
    run = jnp.zeros((HD, HD), F32)
    run_len = jnp.zeros((1, HD), F32)
    pre_state, pre_len = run, run_len
    for g in range(4):
        pre_state = jnp.where(b == g, run, pre_state)
        pre_len = jnp.where(b == g, run_len, pre_len)
        tail = sx[g, pl.ds(HD, 16), :].astype(F32)
        length = tail[0:1] + tail[1:2]
        run = run * jnp.exp2(length) + sx[g, pl.ds(0, HD), :].astype(F32)
        run_len = run_len + length
    sz[a, pl.ds(0, HD), :] = run.astype(BF16)
    sz[a, pl.ds(HD, 16), :] = rows_of(split(run_len))
    for d in range(1, 4):

        @pl.when(a + d <= 3)
        def _():
            remote(sz.at[a], sz.at[a], M_SZ + d, z=a + d).start()

    arrived(kbuf.at[xo], M_K + 4)
    arrived(vbuf.at[xo], M_K + 5)
    pairs(xo, jnp.where(xo < b, 0, 1))

    def joined(d):
        total = jnp.zeros((TOK, HD), F32)
        behind = jnp.zeros((TOK, HD), F32)
        for g in range(3, -1, -1):
            total = total + jnp.exp2(-behind) * pbuf[g, d]
            behind = behind + tbuf[g, d]
        return total, behind

    for d in (2, 3, 1):

        @pl.when(a + d <= 3)
        def _():
            total, behind = joined(d)
            sbuf[d, pl.ds(0, TOK), :] = total.astype(BF16)
            lines = [jnp.transpose(behind[128 * r : 128 * r + 128])[0:1] for r in range(CH)]
            parts = [split(line) for line in lines]
            sbuf[d, pl.ds(TOK, 16), :] = rows_of([p[0] for p in parts] + [p[1] for p in parts])
            remote(sbuf.at[d], rbuf.at[d], M_PO + d, z=a + d).start()

    for d in range(1, 4):

        @pl.when(a >= d)
        def _():
            arrived(sz.at[a - d], M_SZ + d)

    def add_group(g, carried):
        tail = sz[g, pl.ds(HD, 16), :].astype(F32)
        return carried * jnp.exp2(tail[0:1] + tail[1:2]) + sz[g, pl.ds(0, HD), :].astype(F32)

    older = lax.fori_loop(0, a, add_group, jnp.zeros((HD, HD), F32))
    incoming = pre_state + older * jnp.exp2(pre_len)
    raw = lacc[...] + nt(qx[...], incoming.astype(BF16))
    lngl.wait()
    normed = raw * lax.rsqrt(jnp.mean(raw * raw, axis=1, keepdims=True) + EPS) * lng[...]
    gate = lg[...].astype(F32)
    linb[...] = (normed * (gate / (1.0 + jnp.exp2(gate * (-LOG2E))))).astype(BF16)

    def span(r):
        return pl.ds(pl.multiple_of(OUT_ROWS * r, 16), OUT_ROWS)

    def exchange(src, dst, first):
        for k in range(1, 8):
            r = lax.rem(tp + k, 8)
            send(src.at[span(r)], dst.at[tp], first + k, y=r // 2, c=lax.rem(r, 2))
        dst[tp] = src[span(tp), :]

    def collected(dst, first):
        for k in range(1, 8):
            arrived(dst.at[lax.rem(tp + 8 - k, 8)], first + k)
        return jnp.concatenate([dst[i] for i in range(8)], axis=1)

    exchange(linb, xl, M_LA)
    total, behind = joined(0)
    stk[...] = total
    ctot[...] = behind
    oll.wait()
    lhs = collected(xl, M_LA)
    for n in range(4):
        cols = pl.ds(512 * n, 512)
        oacc[:, cols] = mm(lhs, ol[:, cols])

    for d in range(1, 4):

        @pl.when(a >= d)
        def _():
            arrived(rbuf.at[d], M_PO + d)
            stk[...] += jnp.exp2(-ctot[...]) * rbuf[d, pl.ds(0, TOK), :].astype(F32)
            if d < 3:
                tail = rbuf[d, pl.ds(TOK, 16), :].astype(F32)
                for r in range(CH):
                    line = tail[r : r + 1] + tail[CH + r : CH + r + 1]
                    ctot[pl.ds(128 * r, 128), :] += jnp.transpose(jnp.broadcast_to(line, (128, 128)))

    stb[...] = stk[...].astype(BF16)
    exchange(stb, xs, M_ST)
    osl.wait()
    lhs = collected(xs, M_ST)
    for n in range(4):
        cols = pl.ds(512 * n, 512)
        out[:, cols] = (oacc[:, cols] + mm(lhs, os_[:, cols])).astype(BF16)

    for src, i in started:
        sent(src, i)
    for d in range(1, 4):

        @pl.when(a >= d)
        def _():
            sent(qbuf.at[0], M_Q + d)

        @pl.when(a + d <= 3)
        def _():
            sent(sz.at[a], M_SZ + d)
            sent(sbuf.at[d], M_PO + d)


def per_device(*args):
    args = list(args)
    args[1] = args[1].astype(F32).reshape(16, 128)
    args[9] = args[9].reshape(1, HD)
    vm = pltpu.VMEM
    return pl.pallas_call(
        kernel,
        out_shape=jax.ShapeDtypeStruct((OUT_ROWS, D), BF16),
        in_specs=[pl.BlockSpec(memory_space=pl.ANY)] * 16,
        out_specs=pl.BlockSpec(memory_space=pltpu.VMEM),
        scratch_shapes=[
            vm((16, TOK, 128), BF16),
            vm((D, 1024), BF16),
            vm((D, 32), BF16),
            vm((32, 128), BF16),
            vm((16, 128), F32),
            vm((TOK, 1024), F32),
            vm((TOK, 128), F32),
            vm((TOK, 128), F32),
            vm((1, TOK), BF16),
            vm((1, 128), F32),
            vm((1024, D), BF16),
            vm((1024, D), BF16),
            vm((128 * (LEVELS + 2), 128), BF16),
            vm((256, 256), BF16),
            vm((4, TOK + 16, 128), BF16),
            vm((4, TOK, 128), BF16),
            vm((4, TOK, 128), BF16),
            vm((TOK, 128), BF16),
            vm((TOK, 128), BF16),
            vm((TOK, 128), BF16),
            vm((TOK, 128), BF16),
            vm((TOK, 128), F32),
            vm((TOK, 128), BF16),
            vm((4, 144, 128), BF16),
            vm((4, 144, 128), BF16),
            vm((4, 4, TOK, 128), F32),
            vm((4, 4, TOK, 128), F32),
            vm((4, TOK + 16, 128), BF16),
            vm((4, TOK + 16, 128), BF16),
            vm((TOK, 128), F32),
            vm((TOK, 128), F32),
            vm((TOK, 128), BF16),
            vm((TOK, 128), BF16),
            vm((8, OUT_ROWS, 128), BF16),
            vm((8, OUT_ROWS, 128), BF16),
            vm((OUT_ROWS, D), F32),
            pltpu.SemaphoreType.DMA((17,)),
            pltpu.SemaphoreType.DMA((N_MSG,)),
            pltpu.SemaphoreType.DMA((N_MSG,)),
        ],
        compiler_params=pltpu.CompilerParams(collective_id=0, has_side_effects=True),
        name="layer",
    )(*args)


def solution(mesh):
    torus = Mesh(mesh.devices.reshape(4, 4, 4, 2), ("z", "x", "y", "c"))
    sp, tp = ("z", "x"), ("y", "c")
    placed = (
        P(sp, tp), P(), P(None, tp), P(None, tp), P(None, tp), P(None, tp), P(), P(), P(sp, tp), P(),
        P(None, tp), P(None, tp), P(None, tp), P(tp, sp), P(), P(),
    )
    return jax.shard_map(
        per_device, mesh=torus, in_specs=placed, out_specs=P(sp + tp, None), check_vma=False
    )
```

time: 182 us -> 52.2 us (0.29)
  the two profiles are of different devices: /device:TPU:102 before, /device:TPU:39 now
where the time goes in v1:
time: 52.2 us; the launch traced here: 52.1 us
  Pallas kernels  47.2 us (90%)
  local copies, waits for them, and re-layouts  3.52 us (7%)
  other arithmetic  1.29 us (2%)
    pallas_call x1, Pallas kernels, per_device(): pl.pallas_call(kernel, out_shape=jax.ShapeDtypeStruct((OUT_ROWS, D), BF16...  47.2 us
    unnamed x2, local copies, waits for them, and re-layouts  3.52 us
    reshape x1, other arithmetic, per_device(): args[1] = args[1].astype(F32).reshape(16, 128)  1.29 us

profile of v1, /device:TPU:39, one launch (start us, length us, event | category | flops | bytes accessed | tf_op | source)
XLA Modules:
  0.0 52.1 jit_solution(4342079697677762614)
XLA Ops:
  0.0 1.3 %bitcast_convert_fusion.gain = f32[16,128]{1,0:T(8,128)} fusion(bf16[2048]{0:T(1024)(128)(2,1)} %param.17), kind=kLoop, calls=%fused_computation | loop fusion | flops 2048 | bytes 12288 | tf_op jit(solution)/shard_map/reshape | solution.py:448
  1.3 1.9 %copy.17.w_gd = bf16[2048,32]{1,0:T(8,128)(2,1)} copy(bf16[2048,32]{0,1:T(8,128)(2,1)} %param.22) | data formatting | bytes 262144 | tf_op args[6]
  3.2 47.2 %layer.1 = bf16[48,2048]{1,0:T(8,128)(2,1)} custom-call(bf16[384,256]{1,0:T(8,128)(2,1)} %tokens.1, f32[16,128]{1,0:T(8,128)} %bitcast_convert_fusion.gain, bf16[2048,128]{1,0:T(8,128)(2,1)} %w_lq.1, bf16[2048,128]{1,0:T(8,128)(2,1)} %w_lk.1, bf16[2048,128]{1,0:T(8,128)(2,1)} %w_lv.1, bf16[2048,128]{1,0:T(8,128)(2,1)} %w_lg.1, bf16[2048,32]{1,0:T(8,128)(2,1)} %copy.17.w_gd, ...), custom_call_target="tpu_custom_call" | custom-call | tf_op jit(solution)/shard_map/layer/pallas_call | solution.py:451
  50.4 1.6 %copy.19 = bf16[48,2048]{1,0:T(8,128)(2,1)} copy(bf16[48,2048]{1,0:T(8,128)(2,1)} %layer.1) | data formatting | bytes 393216

commit v2 on v1

v2 whole, which is shorter than its diff:
```python
import jax
import jax.numpy as jnp
from jax import lax
from jax.experimental import pallas as pl
from jax.experimental.pallas import tpu as pltpu
from jax.sharding import Mesh
from jax.sharding import PartitionSpec as P

MESH = pl.DeviceIdType.MESH
F32 = jnp.float32
BF16 = jnp.bfloat16
LOG2E = 1.4426950408889634
EPS = 1e-6
SOFT = 16.0
TOK = 384
D = 2048
HD = 128
PARTS = 3
ROWS = TOK // PARTS
CH = TOK // 128
LEVELS = 7
OUT_ROWS = TOK // 8

M_A0, M_A1, M_B0, M_B1, M_P0, M_C, M_D, M_P1, M_P2, M_P3, M_P4, M_P5, M_P6 = [PARTS * i for i in range(13)]
M_K = 13 * PARTS
M_SX = M_K + 6
M_Q = M_SX + 4
M_SZ = M_Q + 4
M_LA = M_SZ + 4
M_R = M_LA + 8
N_MSG = M_R + 32


PROFILE = False


class Marks:
    current = None

    def __call__(self, name):
        if not PROFILE:
            return
        if self.current is not None:
            self.current.__exit__(None, None, None)
        self.current = jax.named_scope(name) if name else None
        if name:
            self.current.__enter__()


def nt(a, b):
    return lax.dot_general(a, b, (((1,), (1,)), ((), ())), preferred_element_type=F32)


def tn(a, b):
    return lax.dot_general(a, b, (((0,), (0,)), ((), ())), preferred_element_type=F32)


def mm(a, b):
    return jnp.dot(a, b, preferred_element_type=F32)


def iota(shape, dim):
    return lax.broadcasted_iota(jnp.int32, shape, dim)


def split(x):
    hi = x.astype(BF16)
    return hi, (x - hi.astype(F32)).astype(BF16)


def rows_of(pieces):
    io = iota((16, 128), 0)
    out = jnp.zeros((16, 128), F32)
    for r, piece in enumerate(pieces):
        out = jnp.where(io == r, piece.astype(F32), out)
    return out.astype(BF16)


def kernel(
    tokens, gain, w_lq, w_lk, w_lv, w_lg, w_gd, w_gu, dob, lgain, w_sq, w_sk, w_sv, kbias, w_ol, w_os,
    out,
    tok, wbuf, gd, gu, gb, gf, acc, ss, dbuf, kb, lng, ol, os_,
    mcon, tri, kbuf, vbuf, qbuf, lq, lk, lv, lg, gs, ffrom, fall, sthis, lacc, qx, sx, sz, pbuf, tbuf, sbuf, rbuf,
    linb, xl, oacc,
    lsem, ssem, rsem,
):
    mark = Marks()
    a, b = lax.axis_index("z"), lax.axis_index("x")
    y, c = lax.axis_index("y"), lax.axis_index("c")
    tp = 2 * y + c
    oc = 1 - c
    scale = HD ** (-0.5)

    def local(src, dst, i):
        cp = pltpu.make_async_copy(src, dst, lsem.at[i])
        cp.start()
        return cp

    def remote(src, dst, i, **dev):
        return pltpu.make_async_remote_copy(
            src_ref=src, dst_ref=dst, send_sem=ssem.at[i], recv_sem=rsem.at[i],
            device_id=dev, device_id_type=MESH,
        )

    def arrived(dst, i):
        remote(dst, dst, i, c=oc).wait_recv()

    def sent(src, i):
        remote(src, src, i, c=oc).wait_send()

    started = []

    def send(src, dst, i, **dev):
        remote(src, dst, i, **dev).start()
        started.append((src, i))

    mark("load")
    base = 4 * y + 2 * c
    loads = [
        local(tokens.at[:, pl.ds(0, 128)], tok.at[base], 0),
        local(tokens.at[:, pl.ds(128, 128)], tok.at[base + 1], 1),
    ]
    barrier = pltpu.get_barrier_semaphore()
    for k in range(1, 4):
        pl.semaphore_signal(barrier, inc=1, device_id={"x": lax.rem(b + k, 4)}, device_id_type=MESH)
        pl.semaphore_signal(barrier, inc=1, device_id={"z": lax.rem(a + k, 4)}, device_id_type=MESH)
    for k in range(1, 8):
        r = lax.rem(tp + k, 8)
        pl.semaphore_signal(
            barrier, inc=1, device_id={"y": r // 2, "c": lax.rem(r, 2)}, device_id_type=MESH
        )
    weights = [w_sk, w_sq, w_sv, w_lk, w_lv, None, w_lq, w_lg]
    wloads = [
        local(w, wbuf.at[:, pl.ds(128 * i, 128)], 2 + i) for i, w in enumerate(weights) if w is not None
    ]
    gdl = local(w_gd, gd, 7)
    gainl = local(gain, gb, 10)
    kbl = local(kbias, kb, 11)
    gul = local(w_gu.at[:, pl.ds(pl.multiple_of(128 * tp, 128), 128)], gu, 12)
    dobl = local(dob, dbuf, 13)
    lngl = local(lgain, lng, 14)
    oll = local(w_ol, ol, 15)
    osl = local(w_os, os_, 16)

    t_i, s_i = iota((128, 128), 0), iota((128, 128), 1)
    mcon[pl.ds(0, 128), :] = jnp.where(s_i <= t_i, 1.0, 0.0).astype(BF16)
    mcon[pl.ds(128, 128), :] = jnp.where(s_i > t_i, 1.0, 0.0).astype(BF16)
    mark("barrier")
    for cp in loads:
        cp.wait()
    pl.semaphore_wait(barrier, 13)

    mark("send")
    yp, ym, yo = lax.rem(y + 1, 4), lax.rem(y + 3, 4), lax.rem(y + 2, 4)

    def part(first, count, r):
        return tok.at[pl.ds(first, count), pl.ds(ROWS * r, ROWS), :]

    def send_part(first, count, r, m, **dev):
        ref = part(first, count, r)
        send(ref, ref, m + r, **dev)

    for r in range(PARTS):
        send_part(base, 1, r, M_A0, y=yp)
        send_part(base + 1, 1, r, M_B1, y=ym)
    for r in range(PARTS):
        send_part(base, 2, r, M_P0, c=oc)
    send_part(base + 1, 1, 0, M_A1, y=yp)
    send_part(base, 1, 0, M_B0, y=ym)

    for lev in range(LEVELS):
        same = (t_i >> lev) == (s_i >> lev)
        second = ((t_i >> lev) & 1) == 1
        m = jnp.where(same, jnp.where(second, jnp.where(s_i <= t_i, 1.0, 0.0), jnp.where(s_i > t_i, 1.0, 0.0)), 0.0)
        mcon[pl.ds(256 + 128 * lev, 128), :] = m.astype(BF16)
    tri[...] = jnp.where(iota((256, 256), 0) > iota((256, 256), 1), 1.0, 0.0).astype(BF16)
    for g in range(4):
        pbuf[g, 0] = jnp.zeros((TOK, HD), F32)
        tbuf[g, 0] = jnp.zeros((TOK, HD), F32)
    gainl.wait()
    gf[...] = gb[...].astype(F32)
    kbl.wait()
    kbuf[b, pl.ds(TOK, 16), :] = rows_of([kb[:, pl.ds(128 * r, 128)] for r in range(CH)])
    gdl.wait()
    for i in range(16):
        down = gd[:, pl.ds(128 * i, 128)].astype(F32)
        square = jnp.concatenate([down, jnp.zeros((96, 128), F32)], axis=0)
        wbuf[pl.ds(128 * i, 128), pl.ds(640, 128)] = jnp.transpose(square).astype(BF16)
    for cp in wloads:
        cp.wait()

    def scaled(chip, first=False):
        pieces = []
        for j in range(4):
            x = tok[4 * chip + j].astype(F32)
            sq = x * x
            ss[...] = sq if (first and j == 0) else ss[...] + sq
            pieces.append((x * gf[pl.ds(4 * chip + j, 1), :]).astype(BF16))
        return jnp.concatenate(pieces, axis=1)

    def weight_rows(chip):
        return pl.ds(pl.multiple_of(512 * chip, 512), 512)

    def fold(chip, first=False):
        lhs = scaled(chip, first)
        for n in range(4):
            cols = pl.ds(256 * n, 256)
            add = mm(lhs, wbuf[weight_rows(chip), cols])
            acc[:, cols] = add if first else acc[:, cols] + add

    mark("own")
    for r in range(PARTS):
        arrived(part(4 * y + 2 * oc, 2, r), M_P0 + r)
    fold(y, True)
    mark("fwd")
    for r in range(PARTS):
        arrived(part(4 * ym + 2 * c, 1, r), M_A0 + r)
        send_part(4 * ym + 2 * c, 1, r, M_C, y=yp)
        arrived(part(4 * yp + 2 * c + 1, 1, r), M_B1 + r)
        send_part(4 * yp + 2 * c + 1, 1, r, M_D, y=ym)
        if r + 1 < PARTS:
            send_part(base + 1, 1, r + 1, M_A1, y=yp)
            send_part(base, 1, r + 1, M_B0, y=ym)
        send_part(4 * ym + 2 * c, 1, r, M_P1, c=oc)
        send_part(4 * yp + 2 * c + 1, 1, r, M_P2, c=oc)
    mark("fwd1")
    for r in range(PARTS):
        arrived(part(4 * ym + 2 * c + 1, 1, r), M_A1 + r)
        send_part(4 * ym + 2 * c + 1, 1, r, M_P3, c=oc)
        arrived(part(4 * yp + 2 * c, 1, r), M_B0 + r)
        send_part(4 * yp + 2 * c, 1, r, M_P4, c=oc)
        if r + 1 < PARTS:
            arrived(part(4 * yo + 2 * c, 1, r), M_C + r)
            send_part(4 * yo + 2 * c, 1, r, M_P5, c=oc)
            arrived(part(4 * yo + 2 * c + 1, 1, r), M_D + r)
            send_part(4 * yo + 2 * c + 1, 1, r, M_P6, c=oc)
    mark("fold2")
    for r in range(PARTS):
        arrived(part(4 * ym + 2 * oc, 1, r), M_P1 + r)
        arrived(part(4 * ym + 2 * oc + 1, 1, r), M_P3 + r)
    fold(ym)
    r = PARTS - 1
    arrived(part(4 * yo + 2 * c, 1, r), M_C + r)
    send_part(4 * yo + 2 * c, 1, r, M_P5, c=oc)
    arrived(part(4 * yo + 2 * c + 1, 1, r), M_D + r)
    send_part(4 * yo + 2 * c + 1, 1, r, M_P6, c=oc)
    for r in range(PARTS):
        arrived(part(4 * yp + 2 * oc, 1, r), M_P4 + r)
        arrived(part(4 * yp + 2 * oc + 1, 1, r), M_P2 + r)
    fold(yp)
    mark("fwd2")
    for r in range(PARTS):
        arrived(part(4 * yo + 2 * oc, 1, r), M_P5 + r)
        arrived(part(4 * yo + 2 * oc + 1, 1, r), M_P6 + r)

    mark("finish")
    lhs = scaled(yo)
    inv = lax.rsqrt(jnp.sum(ss[...], axis=1, keepdims=True) * (1.0 / D) + EPS)

    def finish(n):
        cols = pl.ds(256 * n, 256)
        total = acc[:, cols] + mm(lhs, wbuf[weight_rows(yo), cols])
        return (total * inv).astype(BF16)

    xp, xm, xo = lax.rem(b + 1, 4), lax.rem(b + 3, 4), lax.rem(b + 2, 4)
    got = finish(0)
    kbuf[b, pl.ds(0, TOK), :] = got[:, :128]
    qbuf[0] = got[:, 128:]
    send(kbuf.at[b], kbuf.at[b], M_K, x=xp)
    send(kbuf.at[b], kbuf.at[b], M_K + 1, x=xm)

    @pl.when(a >= 1)
    def _():
        remote(qbuf.at[0], qbuf.at[1], M_Q + 1, z=a - 1).start()

    @pl.when(a == 3)
    def _():
        remote(qbuf.at[0], qbuf.at[3], M_Q + 3, z=0).start()

    got = finish(1)
    vbuf[b] = got[:, :128]
    lk[...] = got[:, 128:]
    send(vbuf.at[b], vbuf.at[b], M_K + 3, x=xm)
    send(vbuf.at[b], vbuf.at[b], M_K + 2, x=xp)
    got = finish(2)
    lv[...] = got[:, :128]
    low = got[:, 128:160]
    got = finish(3)
    lq[...] = got[:, :128]
    lg[...] = got[:, 128:]

    mark("lstate")
    gul.wait()
    dobl.wait()
    pre = (mm(low, gu[...]) + dbuf[...]) * LOG2E
    decay = (jnp.minimum(pre, 0.0) - jnp.log2(1.0 + jnp.exp2(-jnp.abs(pre)))) * (1.0 / SOFT)
    ghi, glo = split(decay)
    gboth = jnp.concatenate([ghi, glo], axis=1)
    gs[...] = gboth
    state = jnp.zeros((HD, HD), F32)
    before = jnp.zeros((1, HD), F32)
    for n in range(CH):
        rows = slice(128 * n, 128 * n + 128)
        both = mm(mcon[pl.ds(0, 256), :], gboth[rows])
        dist = both[:, :128] + both[:, 128:]
        fade = jnp.exp2(dist)
        ffrom[rows, :] = fade[:128]
        fall[rows, :] = fade[:128] * jnp.exp2(before)
        if n:
            sthis[n] = state.astype(BF16)
        length = dist[127:128]
        ke = (lk[rows, :].astype(F32) * fade[128:]).astype(BF16)
        state = state * jnp.exp2(length) + tn(lv[rows, :], ke)
        before = before + length
    sx[b, pl.ds(0, HD), :] = state.astype(BF16)
    sx[b, pl.ds(HD, 16), :] = rows_of(split(before))
    for k in range(1, 4):
        send(sx.at[b], sx.at[b], M_SX + k, x=lax.rem(b + k, 4))

    def linear_inside():
        apart = t_i ^ s_i
        for n in range(CH):
            rows = slice(128 * n, 128 * n + 128)
            both = mm(mcon[pl.ds(256, 128 * LEVELS), :], gs[rows, :])
            fade = jnp.exp2(both[:, :128] + both[:, 128:])
            qh, kh, vh = lq[rows, :], lk[rows, :], lv[rows, :]
            qf, kf = qh.astype(F32) * scale, kh.astype(F32)
            score = jnp.where(apart == 0, nt(qh, kh) * scale, 0.0)
            for lev in range(LEVELS):
                e = fade[128 * lev : 128 * lev + 128]
                part_score = nt((qf * e).astype(BF16), (kf * e).astype(BF16))
                score = jnp.where(((apart >> lev) == 1) & (t_i > s_i), part_score, score)
            inner = mm(score.astype(BF16), vh)
            if n:
                inner = inner + nt((qf * ffrom[rows, :]).astype(BF16), sthis[n])
            lacc[rows, :] = inner
            qx[rows, :] = (qf * fall[rows, :]).astype(BF16)

    mark("diag")
    def bias_of(g):
        head = kbuf[g, pl.ds(TOK, 16), :].astype(F32) * LOG2E
        return jnp.concatenate([head[r : r + 1] for r in range(CH)], axis=1)

    def pair(d, g, diagonal=False):
        z = nt(qbuf[d], kbuf[g, pl.ds(0, TOK), :]) * (scale * LOG2E) + bias_of(g)
        soft = jnp.maximum(jnp.log2(1.0 + jnp.exp2(jnp.minimum(z, 126.0))), z)
        own = z - soft
        if diagonal:
            seen = iota((TOK, TOK), 1) < iota((TOK, TOK), 0)
            soft = jnp.where(seen, soft, 0.0)
        sb = soft.astype(BF16)
        near = mm(sb[:, 256:], tri[pl.ds(0, 128), pl.ds(0, 128)])
        near_total = near[:, :1] + soft[:, 256:257]
        far = mm(sb[:, :256], tri[...]) + near_total
        whole = far[:, :1] + soft[:, :1]
        share = jnp.exp2(own - jnp.concatenate([far, near], axis=1))
        if diagonal:
            share = jnp.where(seen, share, 0.0)
        pbuf[g, d] = mm(share.astype(BF16), vbuf[g])
        tbuf[g, d] = jnp.broadcast_to(whole, (TOK, HD))

    pair(0, b, True)

    mark("linear1")

    @pl.when(a >= 1)
    def _():
        linear_inside()

    mark("qwait")

    @pl.when(a <= 2)
    def _():
        arrived(qbuf.at[1], M_Q + 1)

    @pl.when((a >= 1) & (a <= 2))
    def _():
        remote(qbuf.at[1], qbuf.at[2], M_Q + 2, z=a - 1).start()

    @pl.when(a <= 2)
    def _():
        pair(1, b)

    mark("kvwait")
    arrived(kbuf.at[xm], M_K)
    send(kbuf.at[xm], kbuf.at[xm], M_K + 4, x=xp)
    arrived(kbuf.at[xp], M_K + 1)
    arrived(vbuf.at[xp], M_K + 3)
    send(vbuf.at[xp], vbuf.at[xp], M_K + 5, x=xm)
    arrived(vbuf.at[xm], M_K + 2)

    mark("pairs1")

    def both_pairs(d, carry):
        pair(d, xm)
        pair(d, xp)
        return carry

    lax.fori_loop(0, jnp.where(a <= 2, 2, 1), both_pairs, 0)

    mark("states")
    for k in range(1, 4):
        arrived(sx.at[lax.rem(b + 4 - k, 4)], M_SX + k)
    run = jnp.zeros((HD, HD), F32)
    run_len = jnp.zeros((1, HD), F32)
    pre_state, pre_len = run, run_len
    for g in range(4):
        pre_state = jnp.where(b == g, run, pre_state)
        pre_len = jnp.where(b == g, run_len, pre_len)
        tail = sx[g, pl.ds(HD, 16), :].astype(F32)
        length = tail[0:1] + tail[1:2]
        run = run * jnp.exp2(length) + sx[g, pl.ds(0, HD), :].astype(F32)
        run_len = run_len + length
    sz[a, pl.ds(0, HD), :] = run.astype(BF16)
    sz[a, pl.ds(HD, 16), :] = rows_of(split(run_len))
    for d in range(1, 4):

        @pl.when(a + d <= 3)
        def _():
            remote(sz.at[a], sz.at[a], M_SZ + d, z=a + d).start()

    mark("pairs2")
    for d in (3, 2):

        @pl.when(a + d <= 3)
        def _():
            arrived(qbuf.at[d], M_Q + d)
            pair(d, b)

    lax.fori_loop(2, jnp.where(a <= 1, 4 - a, 2), both_pairs, 0)
    mark("kvwait2")
    arrived(kbuf.at[xo], M_K + 4)
    arrived(vbuf.at[xo], M_K + 5)
    mark("pairs3")

    lane = iota((16, 128), 1)

    def hand_on(d):
        total = jnp.zeros((TOK, HD), F32)
        behind = jnp.zeros((TOK, HD), F32)
        for g in range(3, -1, -1):
            counts = (g <= b) if d == 0 else True
            weight = jnp.exp2(-behind)
            total = total + (jnp.where(counts, weight * pbuf[g, d], 0.0) if d == 0 else weight * pbuf[g, d])
            behind = behind + (jnp.where(counts, tbuf[g, d], 0.0) if d == 0 else tbuf[g, d])
        tiles = []
        for r in range(CH):
            line = jnp.transpose(behind[128 * r : 128 * r + 128])[0:1]
            tiles.append(rows_of(split(line)).astype(F32))
        for r in range(8):
            j, o = (OUT_ROWS * r) // 128, (OUT_ROWS * r) % 128
            tail = pltpu.roll(tiles[j], 128 - o, 1) if o else tiles[j]
            if o + OUT_ROWS > 128:
                tail = jnp.where(lane < 128 - o, tail, pltpu.roll(tiles[j + 1], 128 - o, 1))
            sbuf[d, r, pl.ds(0, OUT_ROWS), :] = total[OUT_ROWS * r : OUT_ROWS * r + OUT_ROWS].astype(BF16)
            sbuf[d, r, pl.ds(OUT_ROWS, 16), :] = tail.astype(BF16)
        for k in range(8):
            r = lax.rem(tp + k, 8)
            if d == 0 and k == 0:
                rbuf[0, tp] = sbuf[0, tp]
            else:
                dev = {"y": r // 2, "c": lax.rem(r, 2)}
                if d:
                    dev["z"] = a + d
                remote(sbuf.at[d, r], rbuf.at[d, tp], M_R + 8 * d + k, **dev).start()

    for d in (2, 3, 1):

        @pl.when(a + d <= 3)
        def _():
            pair(d, xo)
            hand_on(d)

    @pl.when(xo < b)
    def _():
        pair(0, xo)

    hand_on(0)
    mark("linear2")

    @pl.when(a == 0)
    def _():
        linear_inside()

    mark("linfin")
    for d in range(1, 4):

        @pl.when(a >= d)
        def _():
            arrived(sz.at[a - d], M_SZ + d)

    def add_group(g, carried):
        tail = sz[g, pl.ds(HD, 16), :].astype(F32)
        return carried * jnp.exp2(tail[0:1] + tail[1:2]) + sz[g, pl.ds(0, HD), :].astype(F32)

    older = lax.fori_loop(0, a, add_group, jnp.zeros((HD, HD), F32))
    incoming = pre_state + older * jnp.exp2(pre_len)
    raw = lacc[...] + nt(qx[...], incoming.astype(BF16))
    lngl.wait()
    normed = raw * lax.rsqrt(jnp.mean(raw * raw, axis=1, keepdims=True) + EPS) * lng[...]
    gate = lg[...].astype(F32)
    linb[...] = (normed * (gate / (1.0 + jnp.exp2(gate * (-LOG2E))))).astype(BF16)

    def span(r):
        return pl.ds(pl.multiple_of(OUT_ROWS * r, 16), OUT_ROWS)

    mark("linx")
    for k in range(1, 8):
        r = lax.rem(tp + k, 8)
        send(linb.at[span(r)], xl.at[tp], M_LA + k, y=r // 2, c=lax.rem(r, 2))
    xl[tp] = linb[span(tp), :]
    oll.wait()
    for k in range(1, 8):
        arrived(xl.at[lax.rem(tp + 8 - k, 8)], M_LA + k)
    mark("linproj")
    lhs = jnp.concatenate([xl[i] for i in range(8)], axis=1)
    for n in range(4):
        cols = pl.ds(512 * n, 512)
        oacc[:, cols] = mm(lhs, ol[:, cols])

    mark("ret0")
    osl.wait()
    for k in range(1, 8):
        arrived(rbuf.at[0, lax.rem(tp + 8 - k, 8)], M_R + k)
    mark("ret")
    for d in range(1, 4):

        @pl.when(a >= d)
        def _():
            for k in range(8):
                arrived(rbuf.at[d, lax.rem(tp + 8 - k, 8)], M_R + 8 * d + k)

    mark("stproj")
    sub = iota((8, 128), 0)
    behind = jnp.zeros((8, 128), F32)
    heads = [rbuf[0, i, pl.ds(0, OUT_ROWS), :].astype(F32) for i in range(8)]
    for d in range(1, 4):
        for i in range(8):
            tail = rbuf[d - 1, i, pl.ds(OUT_ROWS, 16), :].astype(F32)
            behind = behind + jnp.where(sub == i, tail[0:1] + tail[1:2], 0.0)
        left = jnp.transpose(jnp.exp2(-behind))
        for i in range(8):
            more = left[:OUT_ROWS, i : i + 1] * rbuf[d, i, pl.ds(0, OUT_ROWS), :].astype(F32)
            heads[i] = heads[i] + jnp.where(a >= d, more, 0.0)
    lhs = jnp.concatenate([h.astype(BF16) for h in heads], axis=1)
    for n in range(4):
        cols = pl.ds(512 * n, 512)
        out[:, cols] = (oacc[:, cols] + mm(lhs, os_[:, cols])).astype(BF16)

    mark("drain")
    for src, i in started:
        sent(src, i)

    @pl.when(a >= 1)
    def _():
        sent(qbuf.at[0], M_Q + 1)

    @pl.when(a == 3)
    def _():
        sent(qbuf.at[0], M_Q + 3)

    @pl.when((a >= 1) & (a <= 2))
    def _():
        sent(qbuf.at[1], M_Q + 2)

    for d in range(4):

        @pl.when(a + d <= 3)
        def _():
            if d:
                sent(sz.at[a], M_SZ + d)
            for k in range(0 if d else 1, 8):
                sent(sbuf.at[d, lax.rem(tp + k, 8)], M_R + 8 * d + k)

    mark("")


def per_device(*args):
    args = list(args)
    args[1] = args[1].reshape(16, 128)
    args[6] = args[6].T
    args[9] = args[9].reshape(1, HD)
    vm = pltpu.VMEM
    return pl.pallas_call(
        kernel,
        out_shape=pltpu.VMEM((OUT_ROWS, D), BF16),
        in_specs=[pl.BlockSpec(memory_space=pl.ANY)] * 16,
        out_specs=pl.BlockSpec(memory_space=pltpu.VMEM),
        scratch_shapes=[
            vm((16, TOK, 128), BF16),
            vm((D, 1024), BF16),
            vm((32, D), BF16),
            vm((32, 128), BF16),
            vm((16, 128), BF16),
            vm((16, 128), F32),
            vm((TOK, 1024), F32),
            vm((TOK, 128), F32),
            vm((TOK, 128), F32),
            vm((1, TOK), BF16),
            vm((1, 128), F32),
            vm((1024, D), BF16),
            vm((1024, D), BF16),
            vm((128 * (LEVELS + 2), 128), BF16),
            vm((256, 256), BF16),
            vm((4, TOK + 16, 128), BF16),
            vm((4, TOK, 128), BF16),
            vm((4, TOK, 128), BF16),
            vm((TOK, 128), BF16),
            vm((TOK, 128), BF16),
            vm((TOK, 128), BF16),
            vm((TOK, 128), BF16),
            vm((TOK, 256), BF16),
            vm((TOK, 128), F32),
            vm((TOK, 128), F32),
            vm((CH, 128, 128), BF16),
            vm((TOK, 128), F32),
            vm((TOK, 128), BF16),
            vm((4, 144, 128), BF16),
            vm((4, 144, 128), BF16),
            vm((4, 4, TOK, 128), F32),
            vm((4, 4, TOK, 128), F32),
            vm((4, 8, OUT_ROWS + 16, 128), BF16),
            vm((4, 8, OUT_ROWS + 16, 128), BF16),
            vm((TOK, 128), BF16),
            vm((8, OUT_ROWS, 128), BF16),
            vm((OUT_ROWS, D), F32),
            pltpu.SemaphoreType.DMA((17,)),
            pltpu.SemaphoreType.DMA((N_MSG,)),
            pltpu.SemaphoreType.DMA((N_MSG,)),
        ],
        compiler_params=pltpu.CompilerParams(collective_id=0, has_side_effects=True),
        name="layer",
    )(*args)


def solution(mesh):
    torus = Mesh(mesh.devices.reshape(4, 4, 4, 2), ("z", "x", "y", "c"))
    sp, tp = ("z", "x"), ("y", "c")
    placed = (
        P(sp, tp), P(), P(None, tp), P(None, tp), P(None, tp), P(None, tp), P(), P(), P(sp, tp), P(),
        P(None, tp), P(None, tp), P(None, tp), P(tp, sp), P(), P(),
    )
    return jax.shard_map(
        per_device, mesh=torus, in_specs=placed, out_specs=P(sp + tp, None), check_vma=False
    )
```

time: 52.2 us -> 44.4 us (0.85)
  the two profiles are of different devices: /device:TPU:39 before, /device:TPU:1 now
where the time goes in v2:
time: 44.4 us; the launch traced here: 44.3 us
  Pallas kernels  43.6 us (98%)
  local copies, waits for them, and re-layouts  0.68 us (2%)
    pallas_call x1, Pallas kernels, per_device(): pl.pallas_call(kernel, out_shape=pltpu.VMEM((OUT_ROWS, D), BF16), in_spec...  43.6 us

profile of v2, /device:TPU:1, one launch (start us, length us, event | category | flops | bytes accessed | tf_op | source)
XLA Modules:
  0.0 44.3 jit_solution(16963409338836646623)
XLA Ops:
  0.0 43.6 %layer.1 = bf16[48,2048]{1,0:T(8,128)(2,1)S(1)} custom-call(bf16[384,256]{1,0:T(8,128)(2,1)} %tokens.1, bf16[16,128]{1,0:T(8,128)(2,1)} %bitcast.4, bf16[2048,128]{1,0:T(8,128)(2,1)} %w_lq.1, bf16[2048,128]{1,0:T(8,128)(2,1)} %w_lk.1, bf16[2048,128]{1,0:T(8,128)(2,1)} %w_lv.1, bf16[2048,128]{1,0:T(8,128)(2,1)} %w_lg.1, bf16[32,2048]{1,0:T(8,128)(2,1)} %bitcast.3, ...), custom_call_target="tpu_custom_call" | custom-call | tf_op jit(solution)/shard_map/layer/pallas_call | solution.py:584
  43.6 0.7 %copy.18 = bf16[48,2048]{1,0:T(8,128)(2,1)} copy(bf16[48,2048]{1,0:T(8,128)(2,1)S(1)} %layer.1) | data formatting | bytes 393216

commit v3 on v2

--- a/solution.py
+++ b/solution.py
@@ -17,15 +17,17 @@
 HD = 128
 PARTS = 3
 ROWS = TOK // PARTS
+KPARTS = 2
+KROWS = TOK // KPARTS
 CH = TOK // 128
 LEVELS = 7
 OUT_ROWS = TOK // 8
 
 M_A0, M_A1, M_B0, M_B1, M_P0, M_C, M_D, M_P1, M_P2, M_P3, M_P4, M_P5, M_P6 = [PARTS * i for i in range(13)]
 M_K = 13 * PARTS
-M_SX = M_K + 6
+M_SX = M_K + 6 * KPARTS
 M_Q = M_SX + 4
-M_SZ = M_Q + 4
+M_SZ = M_Q + 4 * KPARTS
 M_LA = M_SZ + 4
 M_R = M_LA + 8
 N_MSG = M_R + 32
@@ -123,7 +125,15 @@
     barrier = pltpu.get_barrier_semaphore()
     for k in range(1, 4):
         pl.semaphore_signal(barrier, inc=1, device_id={"x": lax.rem(b + k, 4)}, device_id_type=MESH)
-        pl.semaphore_signal(barrier, inc=1, device_id={"z": lax.rem(a + k, 4)}, device_id_type=MESH)
+
+    @pl.when(a <= 2)
+    def _():
+        pl.semaphore_signal(barrier, inc=1, device_id={"z": a + 1}, device_id_type=MESH)
+
+    @pl.when(a == 0)
+    def _():
+        pl.semaphore_signal(barrier, inc=1, device_id={"z": 3}, device_id_type=MESH)
+
     for k in range(1, 8):
         r = lax.rem(tp + k, 8)
         pl.semaphore_signal(
@@ -148,7 +158,7 @@
     mark("barrier")
     for cp in loads:
         cp.wait()
-    pl.semaphore_wait(barrier, 13)
+    pl.semaphore_wait(barrier, 10 + (a + 1) // 2)
 
     mark("send")
     yp, ym, yo = lax.rem(y + 1, 4), lax.rem(y + 3, 4), lax.rem(y + 2, 4)
@@ -253,6 +263,17 @@
         arrived(part(4 * yo + 2 * oc, 1, r), M_P5 + r)
         arrived(part(4 * yo + 2 * oc + 1, 1, r), M_P6 + r)
 
+    xp, xm, xo = lax.rem(b + 1, 4), lax.rem(b + 3, 4), lax.rem(b + 2, 4)
+
+    def krows(g, r):
+        return kbuf.at[g, pl.ds(KROWS * r, KROWS + (16 if r == KPARTS - 1 else 0))]
+
+    def vrows(g, r):
+        return vbuf.at[g, pl.ds(KROWS * r, KROWS)]
+
+    def qrows(d, r):
+        return qbuf.at[d, pl.ds(KROWS * r, KROWS)]
+
     mark("finish")
     lhs = scaled(yo)
     inv = lax.rsqrt(jnp.sum(ss[...], axis=1, keepdims=True) * (1.0 / D) + EPS)
@@ -262,26 +283,29 @@
         total = acc[:, cols] + mm(lhs, wbuf[weight_rows(yo), cols])
         return (total * inv).astype(BF16)
 
-    xp, xm, xo = lax.rem(b + 1, 4), lax.rem(b + 3, 4), lax.rem(b + 2, 4)
     got = finish(0)
     kbuf[b, pl.ds(0, TOK), :] = got[:, :128]
     qbuf[0] = got[:, 128:]
-    send(kbuf.at[b], kbuf.at[b], M_K, x=xp)
-    send(kbuf.at[b], kbuf.at[b], M_K + 1, x=xm)
-
-    @pl.when(a >= 1)
-    def _():
-        remote(qbuf.at[0], qbuf.at[1], M_Q + 1, z=a - 1).start()
-
-    @pl.when(a == 3)
-    def _():
-        remote(qbuf.at[0], qbuf.at[3], M_Q + 3, z=0).start()
+    for r in range(KPARTS):
+        send(krows(b, r), krows(b, r), M_K + r, x=xp)
+        send(krows(b, r), krows(b, r), M_K + KPARTS + r, x=xm)
+
+    for r in range(KPARTS):
+
+        @pl.when(a >= 1)
+        def _():
+            remote(qrows(0, r), qrows(1, r), M_Q + KPARTS + r, z=a - 1).start()
+
+        @pl.when(a == 3)
+        def _():
+            remote(qrows(0, r), qrows(3, r), M_Q + 3 * KPARTS + r, z=0).start()
 
     got = finish(1)
     vbuf[b] = got[:, :128]
     lk[...] = got[:, 128:]
-    send(vbuf.at[b], vbuf.at[b], M_K + 3, x=xm)
-    send(vbuf.at[b], vbuf.at[b], M_K + 2, x=xp)
+    for r in range(KPARTS):
+        send(vrows(b, r), vrows(b, r), M_K + 3 * KPARTS + r, x=xm)
+        send(vrows(b, r), vrows(b, r), M_K + 2 * KPARTS + r, x=xp)
     got = finish(2)
     lv[...] = got[:, :128]
     low = got[:, 128:160]
@@ -361,42 +385,67 @@
 
     pair(0, b, True)
 
+    def pass_keys(r):
+        arrived(krows(xm, r), M_K + r)
+        send(krows(xm, r), krows(xm, r), M_K + 4 * KPARTS + r, x=xp)
+
+    def pass_values(r):
+        arrived(vrows(xp, r), M_K + 3 * KPARTS + r)
+        send(vrows(xp, r), vrows(xp, r), M_K + 5 * KPARTS + r, x=xm)
+
+    def queries(d):
+        for r in range(KPARTS):
+            arrived(qrows(d, r), M_Q + KPARTS * d + r)
+
+    def pass_queries(r):
+        @pl.when(a <= 2)
+        def _():
+            arrived(qrows(1, r), M_Q + KPARTS + r)
+
+        @pl.when((a >= 1) & (a <= 2))
+        def _():
+            remote(qrows(1, r), qrows(2, r), M_Q + 2 * KPARTS + r, z=a - 1).start()
+
     mark("linear1")
-
-    @pl.when(a >= 1)
+    linear_inside()
+    mark("kvfwd")
+    for r in range(KPARTS):
+        pass_queries(r)
+        pass_keys(r)
+    mark("q1")
+
+    @pl.when(a == 0)
     def _():
-        linear_inside()
-
-    mark("qwait")
-
-    @pl.when(a <= 2)
-    def _():
-        arrived(qbuf.at[1], M_Q + 1)
-
-    @pl.when((a >= 1) & (a <= 2))
-    def _():
-        remote(qbuf.at[1], qbuf.at[2], M_Q + 2, z=a - 1).start()
-
-    @pl.when(a <= 2)
+        queries(3)
+        pair(1, b)
+        pair(3, b)
+
+    @pl.when((a == 1) | (a == 2))
     def _():
         pair(1, b)
 
     mark("kvwait")
-    arrived(kbuf.at[xm], M_K)
-    send(kbuf.at[xm], kbuf.at[xm], M_K + 4, x=xp)
-    arrived(kbuf.at[xp], M_K + 1)
-    arrived(vbuf.at[xp], M_K + 3)
-    send(vbuf.at[xp], vbuf.at[xp], M_K + 5, x=xm)
-    arrived(vbuf.at[xm], M_K + 2)
-
-    mark("pairs1")
-
-    def both_pairs(d, carry):
+    for r in range(KPARTS):
+        pass_values(r)
+    for r in range(KPARTS):
+        arrived(krows(xp, r), M_K + KPARTS + r)
+        arrived(vrows(xm, r), M_K + 2 * KPARTS + r)
+    mark("first")
+
+    count = 4 - a
+    ahead = jnp.where(a == 0, 2, 1)
+
+    def turn(i):
+        far = jnp.where(i == 0, 3, jnp.where(i == 3, 0, i))
+        return jnp.where(a == 0, far, jnp.where(i == count - 1, 0, i + 1))
+
+    def ready(i, carry):
+        d = turn(i)
         pair(d, xm)
         pair(d, xp)
         return carry
 
-    lax.fori_loop(0, jnp.where(a <= 2, 2, 1), both_pairs, 0)
+    lax.fori_loop(0, ahead, ready, 0)
 
     mark("states")
     for k in range(1, 4):
@@ -413,36 +462,63 @@
         run_len = run_len + length
     sz[a, pl.ds(0, HD), :] = run.astype(BF16)
     sz[a, pl.ds(HD, 16), :] = rows_of(split(run_len))
-    for d in range(1, 4):
+    for d in (3, 1):
 
         @pl.when(a + d <= 3)
         def _():
             remote(sz.at[a], sz.at[a], M_SZ + d, z=a + d).start()
 
-    mark("pairs2")
-    for d in (3, 2):
-
-        @pl.when(a + d <= 3)
-        def _():
-            arrived(qbuf.at[d], M_Q + d)
-            pair(d, b)
-
-    lax.fori_loop(2, jnp.where(a <= 1, 4 - a, 2), both_pairs, 0)
+    def add_group(g, carried):
+        tail = sz[g, pl.ds(HD, 16), :].astype(F32)
+        return carried * jnp.exp2(tail[0:1] + tail[1:2]) + sz[g, pl.ds(0, HD), :].astype(F32)
+
+    def span(r):
+        return pl.ds(pl.multiple_of(OUT_ROWS * r, 16), OUT_ROWS)
+
+    lngl.wait()
+
+    def linear_out():
+        older = lax.fori_loop(0, a, add_group, jnp.zeros((HD, HD), F32))
+        incoming = pre_state + older * jnp.exp2(pre_len)
+        raw = lacc[...] + nt(qx[...], incoming.astype(BF16))
+        normed = raw * lax.rsqrt(jnp.mean(raw * raw, axis=1, keepdims=True) + EPS) * lng[...]
+        gate = lg[...].astype(F32)
+        linb[...] = (normed * (gate / (1.0 + jnp.exp2(gate * (-LOG2E))))).astype(BF16)
+        for k in range(1, 8):
+            r = lax.rem(tp + k, 8)
+            remote(linb.at[span(r)], xl.at[tp], M_LA + k, y=r // 2, c=lax.rem(r, 2)).start()
+        xl[tp] = linb[span(tp), :]
+
+    mark("lout0")
+
+    @pl.when(a == 0)
+    def _():
+        linear_out()
+
+    mark("q2")
+
+    @pl.when(a <= 1)
+    def _():
+        queries(2)
+        remote(sz.at[a], sz.at[a], M_SZ + 2, z=a + 2).start()
+        pair(2, b)
+
     mark("kvwait2")
-    arrived(kbuf.at[xo], M_K + 4)
-    arrived(vbuf.at[xo], M_K + 5)
-    mark("pairs3")
+    for r in range(KPARTS):
+        arrived(krows(xo, r), M_K + 4 * KPARTS + r)
+        arrived(vrows(xo, r), M_K + 5 * KPARTS + r)
+    mark("serve")
 
     lane = iota((16, 128), 1)
 
-    def hand_on(d):
+    def hand_on(d, home):
         total = jnp.zeros((TOK, HD), F32)
         behind = jnp.zeros((TOK, HD), F32)
         for g in range(3, -1, -1):
-            counts = (g <= b) if d == 0 else True
+            counts = (g <= b) if home else True
             weight = jnp.exp2(-behind)
-            total = total + (jnp.where(counts, weight * pbuf[g, d], 0.0) if d == 0 else weight * pbuf[g, d])
-            behind = behind + (jnp.where(counts, tbuf[g, d], 0.0) if d == 0 else tbuf[g, d])
+            total = total + (jnp.where(counts, weight * pbuf[g, d], 0.0) if home else weight * pbuf[g, d])
+            behind = behind + (jnp.where(counts, tbuf[g, d], 0.0) if home else tbuf[g, d])
         tiles = []
         for r in range(CH):
             line = jnp.transpose(behind[128 * r : 128 * r + 128])[0:1]
@@ -456,59 +532,46 @@
             sbuf[d, r, pl.ds(OUT_ROWS, 16), :] = tail.astype(BF16)
         for k in range(8):
             r = lax.rem(tp + k, 8)
-            if d == 0 and k == 0:
+            if home and k == 0:
                 rbuf[0, tp] = sbuf[0, tp]
             else:
                 dev = {"y": r // 2, "c": lax.rem(r, 2)}
-                if d:
+                if not home:
                     dev["z"] = a + d
                 remote(sbuf.at[d, r], rbuf.at[d, tp], M_R + 8 * d + k, **dev).start()
 
-    for d in (2, 3, 1):
-
-        @pl.when(a + d <= 3)
-        def _():
-            pair(d, xo)
-            hand_on(d)
-
-    @pl.when(xo < b)
-    def _():
-        pair(0, xo)
-
-    hand_on(0)
-    mark("linear2")
+    def serve(i, carry):
+        d = turn(i)
+        pair(d, xo)
+        hand_on(d, False)
+        ready(i + ahead, 0)
+        return carry
+
+    lax.fori_loop(0, count - ahead, serve, 0)
+    mark("home")
 
     @pl.when(a == 0)
     def _():
-        linear_inside()
-
-    mark("linfin")
-    for d in range(1, 4):
-
-        @pl.when(a >= d)
-        def _():
-            arrived(sz.at[a - d], M_SZ + d)
-
-    def add_group(g, carried):
-        tail = sz[g, pl.ds(HD, 16), :].astype(F32)
-        return carried * jnp.exp2(tail[0:1] + tail[1:2]) + sz[g, pl.ds(0, HD), :].astype(F32)
-
-    older = lax.fori_loop(0, a, add_group, jnp.zeros((HD, HD), F32))
-    incoming = pre_state + older * jnp.exp2(pre_len)
-    raw = lacc[...] + nt(qx[...], incoming.astype(BF16))
-    lngl.wait()
-    normed = raw * lax.rsqrt(jnp.mean(raw * raw, axis=1, keepdims=True) + EPS) * lng[...]
-    gate = lg[...].astype(F32)
-    linb[...] = (normed * (gate / (1.0 + jnp.exp2(gate * (-LOG2E))))).astype(BF16)
-
-    def span(r):
-        return pl.ds(pl.multiple_of(OUT_ROWS * r, 16), OUT_ROWS)
-
+        pair(2, xo)
+        hand_on(2, False)
+
+    pair(0, xo)
+    hand_on(0, True)
+    mark("lout1")
+
+    @pl.when(a >= 1)
+    def _():
+        for d in range(1, 4):
+
+            @pl.when(a >= d)
+            def _():
+                arrived(sz.at[a - d], M_SZ + d)
+
+        linear_out()
+
+    for k in range(1, 8):
+        started.append((linb.at[span(lax.rem(tp + k, 8))], M_LA + k))
     mark("linx")
-    for k in range(1, 8):
-        r = lax.rem(tp + k, 8)
-        send(linb.at[span(r)], xl.at[tp], M_LA + k, y=r // 2, c=lax.rem(r, 2))
-    xl[tp] = linb[span(tp), :]
     oll.wait()
     for k in range(1, 8):
         arrived(xl.at[lax.rem(tp + 8 - k, 8)], M_LA + k)
@@ -551,17 +614,19 @@
     for src, i in started:
         sent(src, i)
 
-    @pl.when(a >= 1)
-    def _():
-        sent(qbuf.at[0], M_Q + 1)
-
-    @pl.when(a == 3)
-    def _():
-        sent(qbuf.at[0], M_Q + 3)
-
-    @pl.when((a >= 1) & (a <= 2))
-    def _():
-        sent(qbuf.at[1], M_Q + 2)
+    for r in range(KPARTS):
+
+        @pl.when(a >= 1)
+        def _():
+            sent(qrows(0, r), M_Q + KPARTS + r)
+
+        @pl.when(a == 3)
+        def _():
+            sent(qrows(0, r), M_Q + 3 * KPARTS + r)
+
+        @pl.when((a >= 1) & (a <= 2))
+        def _():
+            sent(qrows(1, r), M_Q + 2 * KPARTS + r)
 
     for d in range(4):
 

time: 44.4 us -> 40.8 us (0.919)
  Pallas kernels: 43.6 us -> 40 us
    pallas_call x1, Pallas kernels: 43.6 us -> 40 us  [per_device(): pl.pallas_call(kernel, out_shape=pltpu.VMEM((OUT_ROWS, D), BF16), in_spec...]
where the time goes in v3:
time: 40.8 us; the launch traced here: 40.7 us
  Pallas kernels  40 us (98%)
  local copies, waits for them, and re-layouts  0.68 us (2%)
    pallas_call x1, Pallas kernels, per_device(): pl.pallas_call(kernel, out_shape=pltpu.VMEM((OUT_ROWS, D), BF16), in_spec...  40 us

profile of v3, /device:TPU:1, one launch (start us, length us, event | category | flops | bytes accessed | tf_op | source)
XLA Modules:
  0.0 40.7 jit_solution(79457881162143188)
XLA Ops:
  0.0 40.0 %layer.1 = bf16[48,2048]{1,0:T(8,128)(2,1)S(1)} custom-call(bf16[384,256]{1,0:T(8,128)(2,1)} %tokens.1, bf16[16,128]{1,0:T(8,128)(2,1)} %bitcast.4, bf16[2048,128]{1,0:T(8,128)(2,1)} %w_lq.1, bf16[2048,128]{1,0:T(8,128)(2,1)} %w_lk.1, bf16[2048,128]{1,0:T(8,128)(2,1)} %w_lv.1, bf16[2048,128]{1,0:T(8,128)(2,1)} %w_lg.1, bf16[32,2048]{1,0:T(8,128)(2,1)} %bitcast.3, ...), custom_call_target="tpu_custom_call" | custom-call | tf_op jit(solution)/shard_map/layer/pallas_call | solution.py:649
  40.0 0.7 %copy.18 = bf16[48,2048]{1,0:T(8,128)(2,1)} copy(bf16[48,2048]{1,0:T(8,128)(2,1)S(1)} %layer.1) | data formatting | bytes 393216

commit v4 on v3

v4 whole, which is shorter than its diff:
```python
import jax
import jax.numpy as jnp
from jax import lax
from jax.experimental import pallas as pl
from jax.experimental.pallas import tpu as pltpu
from jax.sharding import Mesh
from jax.sharding import PartitionSpec as P

MESH = pl.DeviceIdType.MESH
F32 = jnp.float32
BF16 = jnp.bfloat16
LOG2E = 1.4426950408889634
EPS = 1e-6
SOFT = 16.0
TOK = 384
D = 2048
HD = 128
PARTS = 3
ROWS = TOK // PARTS
KPARTS = 2
KROWS = TOK // KPARTS
CH = TOK // 128
LEVELS = 7
TAIL = 8
OUT_ROWS = TOK // 8

S_TOK, S_K, S_V, S_Q, S_SX, S_SZ, S_LA, S_R, N_S = range(9)
R_AB, R_BA, R_CD = 0, PARTS, 2 * PARTS
R_P0, R_PM, R_PP, R_PO, R_KN, R_VN, R_KF, R_VF, R_SX, R_Q2, R_Q3, R_SZ, R_LA = [3 * PARTS + i for i in range(13)]
R_K = R_LA + 1
R_V = R_K + KPARTS
R_Q = R_V + KPARTS
R_R = R_Q + KPARTS
N_R = R_R + 4


PROFILE = False


class Marks:
    current = None

    def __call__(self, name):
        if not PROFILE:
            return
        if self.current is not None:
            self.current.__exit__(None, None, None)
        self.current = jax.named_scope(name) if name else None
        if name:
            self.current.__enter__()


def nt(a, b):
    return lax.dot_general(a, b, (((1,), (1,)), ((), ())), preferred_element_type=F32)


def tn(a, b):
    return lax.dot_general(a, b, (((0,), (0,)), ((), ())), preferred_element_type=F32)


def mm(a, b):
    return jnp.dot(a, b, preferred_element_type=F32)


def iota(shape, dim):
    return lax.broadcasted_iota(jnp.int32, shape, dim)


def split(x):
    hi = x.astype(BF16)
    return hi, (x - hi.astype(F32)).astype(BF16)


def rows_of(pieces):
    io = iota((16, 128), 0)
    out = jnp.zeros((16, 128), F32)
    for r, piece in enumerate(pieces):
        out = jnp.where(io == r, piece.astype(F32), out)
    return out.astype(BF16)


def kernel(
    tokens, gain, w_lq, w_lk, w_lv, w_lg, w_gd, w_gu, dob, lgain, w_sq, w_sk, w_sv, kbias, w_ol, w_os,
    out,
    tok, wbuf, gd, gu, gb, gf, acc, ss, dbuf, kb, lng, ol, os_,
    mcon, tri, kbuf, vbuf, qbuf, lq, lk, lv, lg, gs, ffrom, fall, sthis, lacc, qx, sx, sz, pbuf, tbuf, sbuf, rbuf,
    linb, xl, oacc,
    lsem, ssem, rsem,
):
    mark = Marks()
    a, b = lax.axis_index("z"), lax.axis_index("x")
    y, c = lax.axis_index("y"), lax.axis_index("c")
    tp = 2 * y + c
    oc = 1 - c
    scale = HD ** (-0.5)

    def local(src, dst, i):
        cp = pltpu.make_async_copy(src, dst, lsem.at[i])
        cp.start()
        return cp

    def remote(src, dst, i, j, **dev):
        return pltpu.make_async_remote_copy(
            src_ref=src, dst_ref=dst, send_sem=ssem.at[i], recv_sem=rsem.at[j],
            device_id=dev, device_id_type=MESH,
        )

    def send(src, dst, i, j, **dev):
        remote(src, dst, i, j, **dev).start()

    def arrived(dst, j):
        remote(dst, dst, 0, j, c=oc).wait_recv()

    def sent(src, i):
        remote(src, src, i, 0, c=oc).wait_send()

    mark("load")
    base = 4 * y + 2 * c
    local(tokens.at[:, pl.ds(0, 128)], tok.at[base], 0)
    local(tokens.at[:, pl.ds(128, 128)], tok.at[base + 1], 0)
    barrier = pltpu.get_barrier_semaphore()
    for k in range(1, 4):
        pl.semaphore_signal(barrier, inc=1, device_id={"x": lax.rem(b + k, 4)}, device_id_type=MESH)

    @pl.when(a <= 2)
    def _():
        pl.semaphore_signal(barrier, inc=1, device_id={"z": a + 1}, device_id_type=MESH)

    @pl.when(a == 0)
    def _():
        pl.semaphore_signal(barrier, inc=1, device_id={"z": 3}, device_id_type=MESH)

    for k in range(1, 8):
        r = lax.rem(tp + k, 8)
        pl.semaphore_signal(
            barrier, inc=1, device_id={"y": r // 2, "c": lax.rem(r, 2)}, device_id_type=MESH
        )
    weights = [w_sk, w_sq, w_sv, w_lk, w_lv, None, w_lq, w_lg]
    for i, w in enumerate(weights):
        if w is not None:
            local(w, wbuf.at[:, pl.ds(128 * i, 128)], 1)
    gdl = local(w_gd, gd, 2)
    gainl = local(gain, gb, 3)
    kbl = local(kbias, kb, 4)
    gul = local(w_gu.at[:, pl.ds(pl.multiple_of(128 * tp, 128), 128)], gu, 5)
    dobl = local(dob, dbuf, 6)
    lngl = local(lgain, lng, 7)
    oll = local(w_ol, ol, 8)
    osl = local(w_os, os_, 9)

    t_i, s_i = iota((128, 128), 0), iota((128, 128), 1)
    mcon[pl.ds(0, 128), :] = jnp.where(s_i <= t_i, 1.0, 0.0).astype(BF16)
    mcon[pl.ds(128, 128), :] = jnp.where(s_i > t_i, 1.0, 0.0).astype(BF16)
    mark("barrier")
    own = tok.at[pl.ds(base, 2)]
    pltpu.make_async_copy(own, own, lsem.at[0]).wait()
    pl.semaphore_wait(barrier, 10 + (a + 1) // 2)

    mark("send")
    yp, ym, yo = lax.rem(y + 1, 4), lax.rem(y + 3, 4), lax.rem(y + 2, 4)

    def part(first, count, r):
        return tok.at[pl.ds(first, count), pl.ds(ROWS * r, ROWS), :]

    def send_part(first, count, r, j, **dev):
        ref = part(first, count, r)
        send(ref, ref, S_TOK, j, **dev)

    for r in range(PARTS):
        send_part(base, 1, r, R_AB + r, y=yp)
        send_part(base + 1, 1, r, R_AB + r, y=ym)
    for r in range(PARTS):
        send_part(base, 2, r, R_P0, c=oc)
    send_part(base + 1, 1, 0, R_BA, y=yp)
    send_part(base, 1, 0, R_BA, y=ym)

    for lev in range(LEVELS):
        same = (t_i >> lev) == (s_i >> lev)
        second = ((t_i >> lev) & 1) == 1
        m = jnp.where(same, jnp.where(second, jnp.where(s_i <= t_i, 1.0, 0.0), jnp.where(s_i > t_i, 1.0, 0.0)), 0.0)
        mcon[pl.ds(256 + 128 * lev, 128), :] = m.astype(BF16)
    tri[...] = jnp.where(iota((256, 256), 0) > iota((256, 256), 1), 1.0, 0.0).astype(BF16)
    for g in range(4):
        pbuf[g, 0] = jnp.zeros((TOK, HD), F32)
        tbuf[g, 0] = jnp.zeros((TOK, HD), F32)
    gainl.wait()
    gf[...] = gb[...].astype(F32)
    kbl.wait()
    kbuf[b, pl.ds(TOK, 16), :] = rows_of([kb[:, pl.ds(128 * r, 128)] for r in range(CH)])
    gdl.wait()
    for i in range(16):
        down = gd[:, pl.ds(128 * i, 128)].astype(F32)
        square = jnp.concatenate([down, jnp.zeros((96, 128), F32)], axis=0)
        wbuf[pl.ds(128 * i, 128), pl.ds(640, 128)] = jnp.transpose(square).astype(BF16)
    seven = wbuf.at[:, pl.ds(0, 896)]
    pltpu.make_async_copy(seven, seven, lsem.at[1]).wait()

    def scaled(block, count, first=False):
        pieces = []
        for j in range(count):
            x = tok[block + j].astype(F32)
            sq = x * x
            ss[...] = sq if (first and j == 0) else ss[...] + sq
            pieces.append((x * gf[pl.ds(block + j, 1), :]).astype(BF16))
        return jnp.concatenate(pieces, axis=1)

    def weight_rows(block, count):
        return pl.ds(pl.multiple_of(128 * block, 256), 128 * count)

    def fold_blocks(block, count, first=False):
        lhs = scaled(block, count, first)
        for n in range(4):
            cols = pl.ds(256 * n, 256)
            add = mm(lhs, wbuf[weight_rows(block, count), cols])
            acc[:, cols] = add if first else acc[:, cols] + add

    def fold(chip, first=False):
        fold_blocks(4 * chip, 4, first)

    def fold_half(chip, core):
        fold_blocks(4 * chip + 2 * core, 2)

    mark("own")

    def partner(chip, j):
        arrived(tok.at[pl.ds(4 * chip + 2 * oc, 2)], j)

    def pass_far(r):
        arrived(part(4 * yo + 2 * c, 2, r), R_CD + r)
        send_part(4 * yo + 2 * c, 2, r, R_PO, c=oc)

    partner(y, R_P0)
    fold(y, True)
    mark("fwd")
    for r in range(PARTS):
        arrived(part(4 * ym + 2 * c, 2, r), R_AB + r)
        send_part(4 * ym + 2 * c, 1, r, R_CD + r, y=yp)
        send_part(4 * yp + 2 * c + 1, 1, r, R_CD + r, y=ym)
        if r + 1 < PARTS:
            send_part(base + 1, 1, r + 1, R_BA + r + 1, y=yp)
            send_part(base, 1, r + 1, R_BA + r + 1, y=ym)
        send_part(4 * ym + 2 * c, 1, r, R_PM, c=oc)
        send_part(4 * yp + 2 * c + 1, 1, r, R_PP, c=oc)
    mark("fwd1")
    for r in range(PARTS):
        arrived(part(4 * ym + 2 * c, 2, r), R_BA + r)
        send_part(4 * ym + 2 * c + 1, 1, r, R_PM, c=oc)
        send_part(4 * yp + 2 * c, 1, r, R_PP, c=oc)
        pass_far(r)
    mark("fold2")
    partner(ym, R_PM)
    fold(ym)
    partner(yp, R_PP)
    fold(yp)
    fold_half(yo, c)
    mark("fwd2")
    partner(yo, R_PO)

    xp, xm, xo = lax.rem(b + 1, 4), lax.rem(b + 3, 4), lax.rem(b + 2, 4)

    def krows(g, r):
        return kbuf.at[g, pl.ds(KROWS * r, KROWS + (16 if r == KPARTS - 1 else 0))]

    def vrows(g, r):
        return vbuf.at[g, pl.ds(KROWS * r, KROWS)]

    def qrows(d, r):
        return qbuf.at[d, pl.ds(KROWS * r, KROWS)]

    mark("finish")
    last = 4 * yo + 2 * oc
    lhs = scaled(last, 2)
    inv = lax.rsqrt(jnp.sum(ss[...], axis=1, keepdims=True) * (1.0 / D) + EPS)

    def finish(n):
        cols = pl.ds(256 * n, 256)
        total = acc[:, cols] + mm(lhs, wbuf[weight_rows(last, 2), cols])
        return (total * inv).astype(BF16)

    got = finish(0)
    kbuf[b, pl.ds(0, TOK), :] = got[:, :128]
    qbuf[0] = got[:, 128:]
    for r in range(KPARTS):
        send(krows(b, r), krows(b, r), S_K, R_K + r, x=xp)
        send(krows(b, r), krows(b, r), S_K, R_KN, x=xm)

    @pl.when(a >= 1)
    def _():
        for r in range(KPARTS):
            send(qrows(0, r), qrows(1, r), S_Q, R_Q + r, z=a - 1)

    @pl.when(a == 3)
    def _():
        send(qbuf.at[0], qbuf.at[3], S_Q, R_Q3, z=0)

    got = finish(1)
    vbuf[b] = got[:, :128]
    lk[...] = got[:, 128:]
    for r in range(KPARTS):
        send(vrows(b, r), vrows(b, r), S_V, R_V + r, x=xm)
        send(vrows(b, r), vrows(b, r), S_V, R_VN, x=xp)
    got = finish(2)
    lv[...] = got[:, :128]
    low = got[:, 128:160]
    got = finish(3)
    lq[...] = got[:, :128]
    lg[...] = got[:, 128:]

    mark("lstate")
    gul.wait()
    dobl.wait()
    pre = (mm(low, gu[...]) + dbuf[...]) * LOG2E
    decay = (jnp.minimum(pre, 0.0) - jnp.log2(1.0 + jnp.exp2(-jnp.abs(pre)))) * (1.0 / SOFT)
    ghi, glo = split(decay)
    gboth = jnp.concatenate([ghi, glo], axis=1)
    gs[...] = gboth
    state = jnp.zeros((HD, HD), F32)
    before = jnp.zeros((1, HD), F32)
    for n in range(CH):
        rows = slice(128 * n, 128 * n + 128)
        both = mm(mcon[pl.ds(0, 256), :], gboth[rows])
        dist = both[:, :128] + both[:, 128:]
        fade = jnp.exp2(dist)
        ffrom[rows, :] = fade[:128]
        fall[rows, :] = fade[:128] * jnp.exp2(before)
        if n:
            sthis[n] = state.astype(BF16)
        length = dist[127:128]
        ke = (lk[rows, :].astype(F32) * fade[128:]).astype(BF16)
        state = state * jnp.exp2(length) + tn(lv[rows, :], ke)
        before = before + length
    sx[b, pl.ds(0, HD), :] = state.astype(BF16)
    sx[b, pl.ds(HD, 16), :] = rows_of(split(before))
    for k in range(1, 4):
        send(sx.at[b], sx.at[b], S_SX, R_SX, x=lax.rem(b + k, 4))

    def linear_inside():
        apart = t_i ^ s_i
        for n in range(CH):
            rows = slice(128 * n, 128 * n + 128)
            both = mm(mcon[pl.ds(256, 128 * LEVELS), :], gs[rows, :])
            fade = jnp.exp2(both[:, :128] + both[:, 128:])
            qh, kh, vh = lq[rows, :], lk[rows, :], lv[rows, :]
            qf, kf = qh.astype(F32) * scale, kh.astype(F32)
            score = jnp.where(apart == 0, nt(qh, kh) * scale, 0.0)
            for lev in range(LEVELS):
                e = fade[128 * lev : 128 * lev + 128]
                part_score = nt((qf * e).astype(BF16), (kf * e).astype(BF16))
                score = jnp.where(((apart >> lev) == 1) & (t_i > s_i), part_score, score)
            inner = mm(score.astype(BF16), vh)
            if n:
                inner = inner + nt((qf * ffrom[rows, :]).astype(BF16), sthis[n])
            lacc[rows, :] = inner
            qx[rows, :] = (qf * fall[rows, :]).astype(BF16)

    mark("diag")
    def bias_of(g):
        head = kbuf[g, pl.ds(TOK, 16), :].astype(F32) * LOG2E
        return jnp.concatenate([head[r : r + 1] for r in range(CH)], axis=1)

    def pair(d, g, diagonal=False):
        z = nt(qbuf[d], kbuf[g, pl.ds(0, TOK), :]) * (scale * LOG2E) + bias_of(g)
        soft = jnp.maximum(jnp.log2(1.0 + jnp.exp2(jnp.minimum(z, 126.0))), z)
        own = z - soft
        if diagonal:
            seen = iota((TOK, TOK), 1) < iota((TOK, TOK), 0)
            soft = jnp.where(seen, soft, 0.0)
        sb = soft.astype(BF16)
        near = mm(sb[:, 256:], tri[pl.ds(0, 128), pl.ds(0, 128)])
        near_total = near[:, :1] + soft[:, 256:257]
        far = mm(sb[:, :256], tri[...]) + near_total
        whole = far[:, :1] + soft[:, :1]
        share = jnp.exp2(own - jnp.concatenate([far, near], axis=1))
        if diagonal:
            share = jnp.where(seen, share, 0.0)
        pbuf[g, d] = mm(share.astype(BF16), vbuf[g])
        tbuf[g, d] = jnp.broadcast_to(whole, (TOK, HD))

    pair(0, b, True)

    def pass_keys(r):
        arrived(krows(xm, r), R_K + r)
        send(krows(xm, r), krows(xm, r), S_K, R_KF, x=xp)

    def pass_values(r):
        arrived(vrows(xp, r), R_V + r)
        send(vrows(xp, r), vrows(xp, r), S_V, R_VF, x=xm)

    def pass_queries(r):
        @pl.when(a <= 2)
        def _():
            arrived(qrows(1, r), R_Q + r)

        @pl.when((a >= 1) & (a <= 2))
        def _():
            send(qrows(1, r), qrows(2, r), S_Q, R_Q2, z=a - 1)

    lane = iota((16, 128), 1)

    def hand_on(d, home):
        total = jnp.zeros((TOK, HD), F32)
        behind = jnp.zeros((TOK, HD), F32)
        for g in range(3, -1, -1):
            counts = (g <= b) if home else True
            weight = jnp.exp2(-behind)
            total = total + (jnp.where(counts, weight * pbuf[g, d], 0.0) if home else weight * pbuf[g, d])
            behind = behind + (jnp.where(counts, tbuf[g, d], 0.0) if home else tbuf[g, d])
        for r in range(8):
            sbuf[8 * d + r, pl.ds(0, OUT_ROWS), :] = total[OUT_ROWS * r : OUT_ROWS * r + OUT_ROWS].astype(BF16)

        def leave(rows):
            for k in range(8):
                r = lax.rem(tp + k, 8)
                if home and k == 0:
                    rbuf[tp] = sbuf[tp]
                else:
                    dev = {"y": r // 2, "c": lax.rem(r, 2)}
                    if not home:
                        dev["z"] = a + d
                    send(sbuf.at[8 * d + r, pl.ds(0, rows)], rbuf.at[8 * d + tp, pl.ds(0, rows)], S_R, R_R + d, **dev)

        @pl.when(a == 0)
        def _():
            leave(OUT_ROWS)

        @pl.when(a > 0)
        def _():
            tiles = []
            for r in range(CH):
                line = jnp.transpose(behind[128 * r : 128 * r + 128])[0:1]
                tiles.append(rows_of(split(line)).astype(F32))
            for r in range(8):
                j, o = (OUT_ROWS * r) // 128, (OUT_ROWS * r) % 128
                tail = pltpu.roll(tiles[j], 128 - o, 1) if o else tiles[j]
                if o + OUT_ROWS > 128:
                    tail = jnp.where(lane < 128 - o, tail, pltpu.roll(tiles[j + 1], 128 - o, 1))
                sbuf[8 * d + r, pl.ds(OUT_ROWS, TAIL), :] = tail[:TAIL].astype(BF16)
            leave(OUT_ROWS + TAIL)

    mark("home0")

    @pl.when(b == 0)
    def _():
        hand_on(0, True)

    mark("linear1")
    linear_inside()
    mark("kvfwd")
    for r in range(KPARTS):
        pass_queries(r)
        pass_keys(r)
    mark("q1")

    @pl.when(a <= 2)
    def _():
        pair(1, b)

    mark("kvwait")
    for r in range(KPARTS):
        pass_values(r)
    arrived(kbuf.at[xp], R_KN)
    arrived(vbuf.at[xm], R_VN)
    mark("first")
    nearest = jnp.where(a <= 2, 1, 0)
    pair(nearest, xm)
    pair(nearest, xp)
    mark("q3")

    @pl.when(a == 0)
    def _():
        arrived(qbuf.at[3], R_Q3)
        pair(3, b)

    mark("states")
    arrived(sx.at[pl.ds(0, 3)], R_SX)
    run = jnp.zeros((HD, HD), F32)
    run_len = jnp.zeros((1, HD), F32)
    pre_state, pre_len = run, run_len
    for g in range(4):
        pre_state = jnp.where(b == g, run, pre_state)
        pre_len = jnp.where(b == g, run_len, pre_len)
        tail = sx[g, pl.ds(HD, 16), :].astype(F32)
        length = tail[0:1] + tail[1:2]
        run = run * jnp.exp2(length) + sx[g, pl.ds(0, HD), :].astype(F32)
        run_len = run_len + length
    sz[a, pl.ds(0, HD), :] = run.astype(BF16)
    sz[a, pl.ds(HD, 16), :] = rows_of(split(run_len))
    for d in (3, 1):

        @pl.when(a + d <= 3)
        def _():
            send(sz.at[a], sz.at[a], S_SZ, R_SZ, z=a + d)

    def add_group(g, carried):
        tail = sz[g, pl.ds(HD, 16), :].astype(F32)
        return carried * jnp.exp2(tail[0:1] + tail[1:2]) + sz[g, pl.ds(0, HD), :].astype(F32)

    def span(r):
        return pl.ds(pl.multiple_of(OUT_ROWS * r, 16), OUT_ROWS)

    lngl.wait()

    def linear_out():
        older = lax.fori_loop(0, a, add_group, jnp.zeros((HD, HD), F32))
        incoming = pre_state + older * jnp.exp2(pre_len)
        raw = lacc[...] + nt(qx[...], incoming.astype(BF16))
        normed = raw * lax.rsqrt(jnp.mean(raw * raw, axis=1, keepdims=True) + EPS) * lng[...]
        gate = lg[...].astype(F32)
        linb[...] = (normed * (gate / (1.0 + jnp.exp2(gate * (-LOG2E))))).astype(BF16)
        for k in range(1, 8):
            r = lax.rem(tp + k, 8)
            send(linb.at[span(r)], xl.at[tp], S_LA, R_LA, y=r // 2, c=lax.rem(r, 2))
        xl[tp] = linb[span(tp), :]

    mark("lout0")

    @pl.when(a == 0)
    def _():
        linear_out()
        pair(3, xm)
        pair(3, xp)

    mark("q2")

    @pl.when(a <= 1)
    def _():
        arrived(qbuf.at[2], R_Q2)
        send(sz.at[a], sz.at[a], S_SZ, R_SZ, z=a + 2)
        pair(2, b)

    @pl.when(a == 1)
    def _():
        pair(2, xm)
        pair(2, xp)

    mark("kvwait2")
    arrived(kbuf.at[xo], R_KF)
    arrived(vbuf.at[xo], R_VF)
    mark("serve")

    other = jnp.where(a == 0, 3, 2)

    @pl.when(a <= 1)
    def _():
        pair(1, xo)
        pair(other, xo)

    @pl.when(a == 2)
    def _():
        pair(1, xo)

    mark("lout1")

    @pl.when(a >= 1)
    def _():
        for d in range(1, 4):

            @pl.when(a == d)
            def _():
                arrived(sz.at[pl.ds(0, d)], R_SZ)

        linear_out()

    mark("hand")

    @pl.when(a <= 1)
    def _():
        hand_on(1, False)
        hand_on(other, False)

    @pl.when(a == 2)
    def _():
        hand_on(1, False)

    mark("home")

    @pl.when((a <= 2) & (b > 0))
    def _():
        pair(0, xm)
        pair(0, xp)
        pair(0, xo)

    @pl.when((a == 3) & (b > 0))
    def _():
        pair(0, xo)

    @pl.when(b > 0)
    def _():
        hand_on(0, True)

    mark("two")

    @pl.when(a == 0)
    def _():
        pair(2, xm)
        pair(2, xp)
        pair(2, xo)
        hand_on(2, False)

    mark("linx")
    oll.wait()
    arrived(xl.at[pl.ds(0, 7)], R_LA)
    mark("linproj")
    lhs = jnp.concatenate([xl[i] for i in range(8)], axis=1)
    for n in range(4):
        cols = pl.ds(512 * n, 512)
        oacc[:, cols] = mm(lhs, ol[:, cols])

    mark("ret0")
    osl.wait()
    def returned(d, first, count):
        @pl.when(a == d)
        def _():
            arrived(rbuf.at[pl.ds(first, count), pl.ds(0, OUT_ROWS)], R_R + d)

        @pl.when(a > d)
        def _():
            arrived(rbuf.at[pl.ds(first, count)], R_R + d)

    returned(0, 0, 7)
    mark("ret")
    for d in range(1, 4):
        returned(d, 8 * d, 8)

    mark("stproj")
    sub = iota((8, 128), 0)
    behind = jnp.zeros((8, 128), F32)
    heads = [rbuf[i, pl.ds(0, OUT_ROWS), :].astype(F32) for i in range(8)]
    for d in range(1, 4):
        for i in range(8):
            tail = rbuf[8 * d - 8 + i, pl.ds(OUT_ROWS, TAIL), :].astype(F32)
            behind = behind + jnp.where(sub == i, tail[0:1] + tail[1:2], 0.0)
        left = jnp.transpose(jnp.exp2(-behind))
        for i in range(8):
            more = left[:OUT_ROWS, i : i + 1] * rbuf[8 * d + i, pl.ds(0, OUT_ROWS), :].astype(F32)
            heads[i] = heads[i] + jnp.where(a >= d, more, 0.0)
    lhs = jnp.concatenate([h.astype(BF16) for h in heads], axis=1)
    for n in range(4):
        cols = pl.ds(512 * n, 512)
        out[:, cols] = (oacc[:, cols] + mm(lhs, os_[:, cols])).astype(BF16)

    mark("drain")
    sent(tok.at[pl.ds(0, 14)], S_TOK)
    sent(kbuf.at[pl.ds(0, 3)], S_K)
    sent(vbuf.at[pl.ds(0, 3)], S_V)
    sent(sx.at[pl.ds(0, 3)], S_SX)
    sent(xl.at[pl.ds(0, 7)], S_LA)

    @pl.when(a >= 1)
    def _():
        sent(qbuf.at[pl.ds(0, 2)], S_Q)

    for d in range(4):

        @pl.when(a == 3 - d)
        def _():
            if d:
                sent(sz.at[pl.ds(0, d)], S_SZ)
            pieces = sbuf.at[pl.ds(0, 7 + 8 * d)]
            sent(pieces if d < 3 else sbuf.at[pl.ds(0, 31), pl.ds(0, OUT_ROWS)], S_R)

    mark("")


def per_device(*args):
    args = list(args)
    args[1] = args[1].reshape(16, 128)
    args[6] = args[6].T
    args[9] = args[9].reshape(1, HD)
    vm = pltpu.VMEM
    return pl.pallas_call(
        kernel,
        out_shape=pltpu.VMEM((OUT_ROWS, D), BF16),
        in_specs=[pl.BlockSpec(memory_space=pl.ANY)] * 16,
        out_specs=pl.BlockSpec(memory_space=pltpu.VMEM),
        scratch_shapes=[
            vm((16, TOK, 128), BF16),
            vm((D, 1024), BF16),
            vm((32, D), BF16),
            vm((32, 128), BF16),
            vm((16, 128), BF16),
            vm((16, 128), F32),
            vm((TOK, 1024), F32),
            vm((TOK, 128), F32),
            vm((TOK, 128), F32),
            vm((1, TOK), BF16),
            vm((1, 128), F32),
            vm((1024, D), BF16),
            vm((1024, D), BF16),
            vm((128 * (LEVELS + 2), 128), BF16),
            vm((256, 256), BF16),
            vm((4, TOK + 16, 128), BF16),
            vm((4, TOK, 128), BF16),
            vm((4, TOK, 128), BF16),
            vm((TOK, 128), BF16),
            vm((TOK, 128), BF16),
            vm((TOK, 128), BF16),
            vm((TOK, 128), BF16),
            vm((TOK, 256), BF16),
            vm((TOK, 128), F32),
            vm((TOK, 128), F32),
            vm((CH, 128, 128), BF16),
            vm((TOK, 128), F32),
            vm((TOK, 128), BF16),
            vm((4, 144, 128), BF16),
            vm((4, 144, 128), BF16),
            vm((4, 4, TOK, 128), F32),
            vm((4, 4, TOK, 128), F32),
            vm((32, OUT_ROWS + TAIL, 128), BF16),
            vm((32, OUT_ROWS + TAIL, 128), BF16),
            vm((TOK, 128), BF16),
            vm((8, OUT_ROWS, 128), BF16),
            vm((OUT_ROWS, D), F32),
            pltpu.SemaphoreType.DMA((10,)),
            pltpu.SemaphoreType.DMA((N_S,)),
            pltpu.SemaphoreType.DMA((N_R,)),
        ],
        compiler_params=pltpu.CompilerParams(collective_id=0, has_side_effects=True),
        name="layer",
    )(*args)


def solution(mesh):
    torus = Mesh(mesh.devices.reshape(4, 4, 4, 2), ("z", "x", "y", "c"))
    sp, tp = ("z", "x"), ("y", "c")
    placed = (
        P(sp, tp), P(), P(None, tp), P(None, tp), P(None, tp), P(None, tp), P(), P(), P(sp, tp), P(),
        P(None, tp), P(None, tp), P(None, tp), P(tp, sp), P(), P(),
    )
    return jax.shard_map(
        per_device, mesh=torus, in_specs=placed, out_specs=P(sp + tp, None), check_vma=False
    )
```

time: 40.8 us -> 35.7 us (0.88)
  the two profiles are of different devices: /device:TPU:1 before, /device:TPU:39 now
where the time goes in v4:
time: 35.7 us; the launch traced here: 35.3 us
  Pallas kernels  34.6 us (97%)
  local copies, waits for them, and re-layouts  0.68 us (2%)
    pallas_call x1, Pallas kernels, per_device(): pl.pallas_call(kernel, out_shape=pltpu.VMEM((OUT_ROWS, D), BF16), in_spec...  34.6 us

profile of v4, /device:TPU:39, one launch (start us, length us, event | category | flops | bytes accessed | tf_op | source)
XLA Modules:
  0.0 35.3 jit_solution(8843254252491679785)
XLA Ops:
  0.0 34.6 %layer.1 = bf16[48,2048]{1,0:T(8,128)(2,1)S(1)} custom-call(bf16[384,256]{1,0:T(8,128)(2,1)} %tokens.1, bf16[16,128]{1,0:T(8,128)(2,1)} %bitcast.4, bf16[2048,128]{1,0:T(8,128)(2,1)} %w_lq.1, bf16[2048,128]{1,0:T(8,128)(2,1)} %w_lk.1, bf16[2048,128]{1,0:T(8,128)(2,1)} %w_lv.1, bf16[2048,128]{1,0:T(8,128)(2,1)} %w_lg.1, bf16[32,2048]{1,0:T(8,128)(2,1)} %bitcast.3, ...), custom_call_target="tpu_custom_call" | custom-call | tf_op jit(solution)/shard_map/layer/pallas_call | solution.py:671
  34.6 0.7 %copy.18 = bf16[48,2048]{1,0:T(8,128)(2,1)} copy(bf16[48,2048]{1,0:T(8,128)(2,1)S(1)} %layer.1) | data formatting | bytes 393216

commit v5 on v4

--- a/solution.py
+++ b/solution.py
@@ -31,7 +31,7 @@
 R_V = R_K + KPARTS
 R_Q = R_V + KPARTS
 R_R = R_Q + KPARTS
-N_R = R_R + 4
+N_R = R_R + 16
 
 
 PROFILE = False
@@ -83,7 +83,7 @@
     tokens, gain, w_lq, w_lk, w_lv, w_lg, w_gd, w_gu, dob, lgain, w_sq, w_sk, w_sv, kbias, w_ol, w_os,
     out,
     tok, wbuf, gd, gu, gb, gf, acc, ss, dbuf, kb, lng, ol, os_,
-    mcon, tri, kbuf, vbuf, qbuf, lq, lk, lv, lg, gs, ffrom, fall, sthis, lacc, qx, sx, sz, pbuf, tbuf, sbuf, rbuf,
+    mcon, tri, kbuf, vbuf, qbuf, lq, lk, lv, lg, gs, ffrom, fall, sthis, lacc, qx, sx, sz, pbuf, tbuf, shares, sbuf, rbuf,
     linb, xl, oacc,
     lsem, ssem, rsem,
 ):
@@ -205,7 +205,7 @@
         return jnp.concatenate(pieces, axis=1)
 
     def weight_rows(block, count):
-        return pl.ds(pl.multiple_of(128 * block, 256), 128 * count)
+        return pl.ds(pl.multiple_of(128 * block, 128), 128 * count)
 
     def fold_blocks(block, count, first=False):
         lhs = scaled(block, count, first)
@@ -216,6 +216,13 @@
 
     def fold(chip, first=False):
         fold_blocks(4 * chip, 4, first)
+
+    def fold_two(one, two):
+        lhs = scaled(one, 1), scaled(two, 1)
+        for n in range(4):
+            cols = pl.ds(256 * n, 256)
+            add = mm(lhs[0], wbuf[weight_rows(one, 1), cols]) + mm(lhs[1], wbuf[weight_rows(two, 1), cols])
+            acc[:, cols] = acc[:, cols] + add
 
     def fold_half(chip, core):
         fold_blocks(4 * chip + 2 * core, 2)
@@ -241,6 +248,8 @@
             send_part(base, 1, r + 1, R_BA + r + 1, y=ym)
         send_part(4 * ym + 2 * c, 1, r, R_PM, c=oc)
         send_part(4 * yp + 2 * c + 1, 1, r, R_PP, c=oc)
+    mark("fold1")
+    fold_two(4 * ym + 2 * c, 4 * yp + 2 * c + 1)
     mark("fwd1")
     for r in range(PARTS):
         arrived(part(4 * ym + 2 * c, 2, r), R_BA + r)
@@ -248,11 +257,13 @@
         send_part(4 * yp + 2 * c, 1, r, R_PP, c=oc)
         pass_far(r)
     mark("fold2")
+    fold_two(4 * ym + 2 * c + 1, 4 * yp + 2 * c)
+    fold_half(yo, c)
+    mark("fold3")
     partner(ym, R_PM)
-    fold(ym)
+    fold_half(ym, oc)
     partner(yp, R_PP)
-    fold(yp)
-    fold_half(yo, c)
+    fold_half(yp, oc)
     mark("fwd2")
     partner(yo, R_PO)
 
@@ -358,7 +369,7 @@
         head = kbuf[g, pl.ds(TOK, 16), :].astype(F32) * LOG2E
         return jnp.concatenate([head[r : r + 1] for r in range(CH)], axis=1)
 
-    def pair(d, g, diagonal=False):
+    def pair(d, g, diagonal=False, slot=None):
         z = nt(qbuf[d], kbuf[g, pl.ds(0, TOK), :]) * (scale * LOG2E) + bias_of(g)
         soft = jnp.maximum(jnp.log2(1.0 + jnp.exp2(jnp.minimum(z, 126.0))), z)
         own = z - soft
@@ -373,8 +384,11 @@
         share = jnp.exp2(own - jnp.concatenate([far, near], axis=1))
         if diagonal:
             share = jnp.where(seen, share, 0.0)
-        pbuf[g, d] = mm(share.astype(BF16), vbuf[g])
         tbuf[g, d] = jnp.broadcast_to(whole, (TOK, HD))
+        if slot is None:
+            pbuf[g, d] = mm(share.astype(BF16), vbuf[g])
+        else:
+            shares[slot] = share.astype(BF16)
 
     pair(0, b, True)
 
@@ -397,7 +411,7 @@
 
     lane = iota((16, 128), 1)
 
-    def hand_on(d, home):
+    def hand_on(d, home, oldest):
         total = jnp.zeros((TOK, HD), F32)
         behind = jnp.zeros((TOK, HD), F32)
         for g in range(3, -1, -1):
@@ -409,39 +423,43 @@
             sbuf[8 * d + r, pl.ds(0, OUT_ROWS), :] = total[OUT_ROWS * r : OUT_ROWS * r + OUT_ROWS].astype(BF16)
 
         def leave(rows):
-            for k in range(8):
-                r = lax.rem(tp + k, 8)
-                if home and k == 0:
-                    rbuf[tp] = sbuf[tp]
-                else:
-                    dev = {"y": r // 2, "c": lax.rem(r, 2)}
+            for far in range(4):
+                for flip in range(2):
+                    to_y, to_c = lax.rem(y + 4 - far, 4), c if flip == 0 else oc
+                    r = 2 * to_y + to_c
+                    if home and far == 0 and flip == 0:
+                        rbuf[tp] = sbuf[tp]
+                        continue
+                    dev = {"y": to_y, "c": to_c}
                     if not home:
                         dev["z"] = a + d
-                    send(sbuf.at[8 * d + r, pl.ds(0, rows)], rbuf.at[8 * d + tp, pl.ds(0, rows)], S_R, R_R + d, **dev)
-
-        @pl.when(a == 0)
-        def _():
+                    src, dst = sbuf.at[8 * d + r, pl.ds(0, rows)], rbuf.at[8 * d + tp, pl.ds(0, rows)]
+                    send(src, dst, S_R, R_R + 4 * d + far, **dev)
+
+        if oldest:
             leave(OUT_ROWS)
-
-        @pl.when(a > 0)
-        def _():
-            tiles = []
-            for r in range(CH):
-                line = jnp.transpose(behind[128 * r : 128 * r + 128])[0:1]
-                tiles.append(rows_of(split(line)).astype(F32))
-            for r in range(8):
-                j, o = (OUT_ROWS * r) // 128, (OUT_ROWS * r) % 128
-                tail = pltpu.roll(tiles[j], 128 - o, 1) if o else tiles[j]
-                if o + OUT_ROWS > 128:
-                    tail = jnp.where(lane < 128 - o, tail, pltpu.roll(tiles[j + 1], 128 - o, 1))
-                sbuf[8 * d + r, pl.ds(OUT_ROWS, TAIL), :] = tail[:TAIL].astype(BF16)
-            leave(OUT_ROWS + TAIL)
+            return
+        tiles = []
+        for r in range(CH):
+            line = jnp.transpose(behind[128 * r : 128 * r + 128])[0:1]
+            tiles.append(rows_of(split(line)).astype(F32))
+        for r in range(8):
+            j, o = (OUT_ROWS * r) // 128, (OUT_ROWS * r) % 128
+            tail = pltpu.roll(tiles[j], 128 - o, 1) if o else tiles[j]
+            if o + OUT_ROWS > 128:
+                tail = jnp.where(lane < 128 - o, tail, pltpu.roll(tiles[j + 1], 128 - o, 1))
+            sbuf[8 * d + r, pl.ds(OUT_ROWS, TAIL), :] = tail[:TAIL].astype(BF16)
+        leave(OUT_ROWS + TAIL)
 
     mark("home0")
 
-    @pl.when(b == 0)
-    def _():
-        hand_on(0, True)
+    @pl.when((b == 0) & (a == 0))
+    def _():
+        hand_on(0, True, True)
+
+    @pl.when((b == 0) & (a > 0))
+    def _():
+        hand_on(0, True, False)
 
     mark("linear1")
     linear_inside()
@@ -449,27 +467,53 @@
     for r in range(KPARTS):
         pass_queries(r)
         pass_keys(r)
-    mark("q1")
+    mark("first")
+    arrived(kbuf.at[xp], R_KN)
 
     @pl.when(a <= 2)
     def _():
         pair(1, b)
+        pair(1, xm, slot=0)
+        pair(1, xp, slot=1)
+
+    @pl.when(a == 3)
+    def _():
+        pair(0, xm, slot=0)
+        pair(0, xp, slot=1)
 
     mark("kvwait")
     for r in range(KPARTS):
         pass_values(r)
-    arrived(kbuf.at[xp], R_KN)
-    arrived(vbuf.at[xm], R_VN)
-    mark("first")
-    nearest = jnp.where(a <= 2, 1, 0)
-    pair(nearest, xm)
-    pair(nearest, xp)
     mark("q3")
 
     @pl.when(a == 0)
     def _():
         arrived(qbuf.at[3], R_Q3)
         pair(3, b)
+
+    arrived(vbuf.at[xm], R_VN)
+
+    def values_in(d):
+        pbuf[xm, d] = mm(shares[0], vbuf[xm])
+        pbuf[xp, d] = mm(shares[1], vbuf[xp])
+
+    mark("more")
+
+    @pl.when(a == 0)
+    def _():
+        values_in(1)
+        pair(3, xm)
+        pair(3, xp)
+        arrived(qbuf.at[2], R_Q2)
+        pair(2, b)
+
+    @pl.when((a == 1) | (a == 2))
+    def _():
+        values_in(1)
+
+    @pl.when(a == 3)
+    def _():
+        values_in(0)
 
     mark("states")
     arrived(sx.at[pl.ds(0, 3)], R_SX)
@@ -491,6 +535,14 @@
         def _():
             send(sz.at[a], sz.at[a], S_SZ, R_SZ, z=a + d)
 
+    @pl.when(a == 1)
+    def _():
+        arrived(qbuf.at[2], R_Q2)
+
+    @pl.when(a <= 1)
+    def _():
+        send(sz.at[a], sz.at[a], S_SZ, R_SZ, z=a + 2)
+
     def add_group(g, carried):
         tail = sz[g, pl.ds(HD, 16), :].astype(F32)
         return carried * jnp.exp2(tail[0:1] + tail[1:2]) + sz[g, pl.ds(0, HD), :].astype(F32)
@@ -514,22 +566,15 @@
 
     mark("lout0")
 
+    @pl.when(a == 1)
+    def _():
+        pair(2, b)
+        pair(2, xm)
+        pair(2, xp)
+
     @pl.when(a == 0)
     def _():
         linear_out()
-        pair(3, xm)
-        pair(3, xp)
-
-    mark("q2")
-
-    @pl.when(a <= 1)
-    def _():
-        arrived(qbuf.at[2], R_Q2)
-        send(sz.at[a], sz.at[a], S_SZ, R_SZ, z=a + 2)
-        pair(2, b)
-
-    @pl.when(a == 1)
-    def _():
         pair(2, xm)
         pair(2, xp)
 
@@ -538,12 +583,17 @@
     arrived(vbuf.at[xo], R_VF)
     mark("serve")
 
-    other = jnp.where(a == 0, 3, 2)
-
-    @pl.when(a <= 1)
+    @pl.when(a == 0)
     def _():
         pair(1, xo)
-        pair(other, xo)
+        pair(3, xo)
+        hand_on(1, False, True)
+        hand_on(3, False, True)
+
+    @pl.when(a == 1)
+    def _():
+        pair(1, xo)
+        pair(2, xo)
 
     @pl.when(a == 2)
     def _():
@@ -563,39 +613,43 @@
 
     mark("hand")
 
-    @pl.when(a <= 1)
-    def _():
-        hand_on(1, False)
-        hand_on(other, False)
+    @pl.when(a == 1)
+    def _():
+        hand_on(1, False, False)
+        hand_on(2, False, False)
 
     @pl.when(a == 2)
     def _():
-        hand_on(1, False)
+        hand_on(1, False, False)
 
     mark("home")
 
-    @pl.when((a <= 2) & (b > 0))
-    def _():
-        pair(0, xm)
-        pair(0, xp)
+    def triple(d):
+        pair(d, xm)
+        pair(d, xp)
+        pair(d, xo)
+
+    @pl.when((a == 0) & (b > 0))
+    def _():
+        pair(2, xo)
+        hand_on(2, False, True)
+        triple(0)
+        hand_on(0, True, True)
+
+    @pl.when((a == 0) & (b == 0))
+    def _():
+        pair(2, xo)
+        hand_on(2, False, True)
+
+    @pl.when(((a == 1) | (a == 2)) & (b > 0))
+    def _():
+        triple(0)
+        hand_on(0, True, False)
+
+    @pl.when((a == 3) & (b > 0))
+    def _():
         pair(0, xo)
-
-    @pl.when((a == 3) & (b > 0))
-    def _():
-        pair(0, xo)
-
-    @pl.when(b > 0)
-    def _():
-        hand_on(0, True)
-
-    mark("two")
-
-    @pl.when(a == 0)
-    def _():
-        pair(2, xm)
-        pair(2, xp)
-        pair(2, xo)
-        hand_on(2, False)
+        hand_on(0, True, False)
 
     mark("linx")
     oll.wait()
@@ -608,36 +662,56 @@
 
     mark("ret0")
     osl.wait()
-    def returned(d, first, count):
+    def returned(d, far):
+        chip = lax.rem(y + far, 4)
+        first, count = (2 * chip, 2) if d or far else (0, 1)
+
         @pl.when(a == d)
         def _():
-            arrived(rbuf.at[pl.ds(first, count), pl.ds(0, OUT_ROWS)], R_R + d)
+            arrived(rbuf.at[pl.ds(8 * d + first, count), pl.ds(0, OUT_ROWS)], R_R + 4 * d + far)
 
         @pl.when(a > d)
         def _():
-            arrived(rbuf.at[pl.ds(first, count)], R_R + d)
-
-    returned(0, 0, 7)
-    mark("ret")
-    for d in range(1, 4):
-        returned(d, 8 * d, 8)
+            arrived(rbuf.at[pl.ds(8 * d + first, count)], R_R + 4 * d + far)
+
+    sub = iota((8, 128), 0)
 
     mark("stproj")
-    sub = iota((8, 128), 0)
-    behind = jnp.zeros((8, 128), F32)
-    heads = [rbuf[i, pl.ds(0, OUT_ROWS), :].astype(F32) for i in range(8)]
-    for d in range(1, 4):
-        for i in range(8):
-            tail = rbuf[8 * d - 8 + i, pl.ds(OUT_ROWS, TAIL), :].astype(F32)
-            behind = behind + jnp.where(sub == i, tail[0:1] + tail[1:2], 0.0)
-        left = jnp.transpose(jnp.exp2(-behind))
-        for i in range(8):
-            more = left[:OUT_ROWS, i : i + 1] * rbuf[8 * d + i, pl.ds(0, OUT_ROWS), :].astype(F32)
-            heads[i] = heads[i] + jnp.where(a >= d, more, 0.0)
-    lhs = jnp.concatenate([h.astype(BF16) for h in heads], axis=1)
-    for n in range(4):
-        cols = pl.ds(512 * n, 512)
-        out[:, cols] = (oacc[:, cols] + mm(lhs, os_[:, cols])).astype(BF16)
+
+    @pl.when(a == 0)
+    def _():
+        for far in (0, 1, 3, 2):
+            returned(0, far)
+            first = 2 * lax.rem(y + far, 4)
+            lhs = jnp.concatenate([rbuf[first + i, pl.ds(0, OUT_ROWS), :] for i in range(2)], axis=1)
+            for n in range(4):
+                cols = pl.ds(512 * n, 512)
+                rows = pl.ds(pl.multiple_of(128 * first, 256), 256)
+                total = oacc[:, cols] + mm(lhs, os_[rows, cols])
+                if far == 2:
+                    out[:, cols] = total.astype(BF16)
+                else:
+                    oacc[:, cols] = total
+
+    @pl.when(a > 0)
+    def _():
+        for far in range(4):
+            for d in range(4):
+                returned(d, far)
+        behind = jnp.zeros((8, 128), F32)
+        heads = [rbuf[i, pl.ds(0, OUT_ROWS), :].astype(F32) for i in range(8)]
+        for d in range(1, 4):
+            for i in range(8):
+                tail = rbuf[8 * d - 8 + i, pl.ds(OUT_ROWS, TAIL), :].astype(F32)
+                behind = behind + jnp.where(sub == i, tail[0:1] + tail[1:2], 0.0)
+            left = jnp.transpose(jnp.exp2(-behind))
+            for i in range(8):
+                more = left[:OUT_ROWS, i : i + 1] * rbuf[8 * d + i, pl.ds(0, OUT_ROWS), :].astype(F32)
+                heads[i] = heads[i] + jnp.where(a >= d, more, 0.0)
+        lhs = jnp.concatenate([h.astype(BF16) for h in heads], axis=1)
+        for n in range(4):
+            cols = pl.ds(512 * n, 512)
+            out[:, cols] = (oacc[:, cols] + mm(lhs, os_[:, cols])).astype(BF16)
 
     mark("drain")
     sent(tok.at[pl.ds(0, 14)], S_TOK)
@@ -706,6 +780,7 @@
             vm((4, 144, 128), BF16),
             vm((4, 4, TOK, 128), F32),
             vm((4, 4, TOK, 128), F32),
+            vm((2, TOK, TOK), BF16),
             vm((32, OUT_ROWS + TAIL, 128), BF16),
             vm((32, OUT_ROWS + TAIL, 128), BF16),
             vm((TOK, 128), BF16),

time: 35.7 us -> 35 us (0.980)
  Pallas kernels: 34.6 us -> 33.9 us
    pallas_call x1, Pallas kernels: 34.6 us -> 33.9 us  [per_device(): pl.pallas_call(kernel, out_shape=pltpu.VMEM((OUT_ROWS, D), BF16), in_spec...]
where the time goes in v5:
time: 35 us; the launch traced here: 34.6 us
  Pallas kernels  33.9 us (97%)
  local copies, waits for them, and re-layouts  0.68 us (2%)
    pallas_call x1, Pallas kernels, per_device(): pl.pallas_call(kernel, out_shape=pltpu.VMEM((OUT_ROWS, D), BF16), in_spec...  33.9 us

profile of v5, /device:TPU:39, one launch (start us, length us, event | category | flops | bytes accessed | tf_op | source)
XLA Modules:
  0.0 34.6 jit_solution(6853444361693962024)
XLA Ops:
  0.0 33.9 %layer.1 = bf16[48,2048]{1,0:T(8,128)(2,1)S(1)} custom-call(bf16[384,256]{1,0:T(8,128)(2,1)} %tokens.1, bf16[16,128]{1,0:T(8,128)(2,1)} %bitcast.4, bf16[2048,128]{1,0:T(8,128)(2,1)} %w_lq.1, bf16[2048,128]{1,0:T(8,128)(2,1)} %w_lk.1, bf16[2048,128]{1,0:T(8,128)(2,1)} %w_lv.1, bf16[2048,128]{1,0:T(8,128)(2,1)} %w_lg.1, bf16[32,2048]{1,0:T(8,128)(2,1)} %bitcast.3, ...), custom_call_target="tpu_custom_call" | custom-call | tf_op jit(solution)/shard_map/layer/pallas_call | solution.py:745
  33.9 0.7 %copy.18 = bf16[48,2048]{1,0:T(8,128)(2,1)} copy(bf16[48,2048]{1,0:T(8,128)(2,1)S(1)} %layer.1) | data formatting | bytes 393216

commit v6 on v5

--- a/solution.py
+++ b/solution.py
@@ -412,13 +412,14 @@
     lane = iota((16, 128), 1)
 
     def hand_on(d, home, oldest):
-        total = jnp.zeros((TOK, HD), F32)
-        behind = jnp.zeros((TOK, HD), F32)
-        for g in range(3, -1, -1):
-            counts = (g <= b) if home else True
-            weight = jnp.exp2(-behind)
-            total = total + (jnp.where(counts, weight * pbuf[g, d], 0.0) if home else weight * pbuf[g, d])
-            behind = behind + (jnp.where(counts, tbuf[g, d], 0.0) if home else tbuf[g, d])
+        def counted(g, value):
+            return jnp.where(g <= b, value, 0.0) if home else value
+
+        total, behind = counted(3, pbuf[3, d]), counted(3, tbuf[3, d])
+        for g in range(2, -1, -1):
+            total = total + counted(g, jnp.exp2(-behind) * pbuf[g, d])
+            if g or not oldest:
+                behind = behind + counted(g, tbuf[g, d])
         for r in range(8):
             sbuf[8 * d + r, pl.ds(0, OUT_ROWS), :] = total[OUT_ROWS * r : OUT_ROWS * r + OUT_ROWS].astype(BF16)
 

time: 35 us -> 35 us (level)
  no operation moved by 1% of the time
where the time goes in v6:
time: 35 us; the launch traced here: 34.6 us
  Pallas kernels  33.9 us (97%)
  local copies, waits for them, and re-layouts  0.68 us (2%)
    pallas_call x1, Pallas kernels, per_device(): pl.pallas_call(kernel, out_shape=pltpu.VMEM((OUT_ROWS, D), BF16), in_spec...  33.9 us

profile of v6, /device:TPU:39, one launch (start us, length us, event | category | flops | bytes accessed | tf_op | source)
XLA Modules:
  0.0 34.6 jit_solution(11291260443200123586)
XLA Ops:
  0.0 33.9 %layer.1 = bf16[48,2048]{1,0:T(8,128)(2,1)S(1)} custom-call(bf16[384,256]{1,0:T(8,128)(2,1)} %tokens.1, bf16[16,128]{1,0:T(8,128)(2,1)} %bitcast.4, bf16[2048,128]{1,0:T(8,128)(2,1)} %w_lq.1, bf16[2048,128]{1,0:T(8,128)(2,1)} %w_lk.1, bf16[2048,128]{1,0:T(8,128)(2,1)} %w_lv.1, bf16[2048,128]{1,0:T(8,128)(2,1)} %w_lg.1, bf16[32,2048]{1,0:T(8,128)(2,1)} %bitcast.3, ...), custom_call_target="tpu_custom_call" | custom-call | tf_op jit(solution)/shard_map/layer/pallas_call | solution.py:746
  33.9 0.7 %copy.18 = bf16[48,2048]{1,0:T(8,128)(2,1)} copy(bf16[48,2048]{1,0:T(8,128)(2,1)S(1)} %layer.1) | data formatting | bytes 393216

commit v7 on v6

--- a/solution.py
+++ b/solution.py
@@ -17,7 +17,7 @@
 HD = 128
 PARTS = 3
 ROWS = TOK // PARTS
-KPARTS = 2
+KPARTS = 1
 KROWS = TOK // KPARTS
 CH = TOK // 128
 LEVELS = 7

time: 35 us -> 34.9 us (level)
  no operation moved by 1% of the time
where the time goes in v7:
time: 34.9 us; the launch traced here: 34.8 us
  Pallas kernels  34.1 us (98%)
  local copies, waits for them, and re-layouts  0.68 us (2%)
    pallas_call x1, Pallas kernels, per_device(): pl.pallas_call(kernel, out_shape=pltpu.VMEM((OUT_ROWS, D), BF16), in_spec...  34.1 us

profile of v7, /device:TPU:39, one launch (start us, length us, event | category | flops | bytes accessed | tf_op | source)
XLA Modules:
  0.0 34.8 jit_solution(5453885950304660246)
XLA Ops:
  0.0 34.1 %layer.1 = bf16[48,2048]{1,0:T(8,128)(2,1)S(1)} custom-call(bf16[384,256]{1,0:T(8,128)(2,1)} %tokens.1, bf16[16,128]{1,0:T(8,128)(2,1)} %bitcast.4, bf16[2048,128]{1,0:T(8,128)(2,1)} %w_lq.1, bf16[2048,128]{1,0:T(8,128)(2,1)} %w_lk.1, bf16[2048,128]{1,0:T(8,128)(2,1)} %w_lv.1, bf16[2048,128]{1,0:T(8,128)(2,1)} %w_lg.1, bf16[32,2048]{1,0:T(8,128)(2,1)} %bitcast.3, ...), custom_call_target="tpu_custom_call" | custom-call | tf_op jit(solution)/shard_map/layer/pallas_call | solution.py:746
  34.1 0.7 %copy.18 = bf16[48,2048]{1,0:T(8,128)(2,1)} copy(bf16[48,2048]{1,0:T(8,128)(2,1)S(1)} %layer.1) | data formatting | bytes 393216
